TPU v7x, 512 devices: a whole 4x4x16 slice. The times are simulated.
512 devices in a mesh: ep: 32 (over z, core), tp: 16 (over y, x).
Axes of the slice: x: 4, y: 4, z: 16, core: 2. Of those that a mesh axis runs over, the one named last changes fastest.
Arguments:
- query_rows: bfloat16 [16384, 2048], P('ep', 'tp'), may hold values from -6 to 6
- key_rows: bfloat16 [16384, 2048], P('ep', 'tp'), may hold values from -6 to 6
- value_rows: bfloat16 [16384, 4096], P('ep', 'tp'), may hold values from -6 to 6
- in_gate: float32 [16, 16384], P('tp', 'ep'), may hold values from -120 to 120
- forget_gate: float32 [16, 16384], P('tp', 'ep'), may hold values from -2 to 20
- out_gate: bfloat16 [16384, 4096], P('ep', 'tp'), may hold values from -6 to 6
- head_gain: float32 [4096], P('tp'), may hold values from 0.1 to 1.9
- mix_weight: bfloat16 [4096, 4096], P(None, 'tp'), may hold values from -0.09375 to 0.09375
- expert_input: bfloat16 [8192, 4096], P('ep', 'tp'), may hold values from -30 to 30
- routes: int32 [8192, 2], P('ep'), may hold values from 0 to 31, all different within a row; in each aligned block of 256 rows (0 to 255, 256 to 511, ...) at most 32 rows name the same one
- route_weight: float32 [8192, 2], P('ep'), may hold values from 0.25 to 1.25
- gate_weight: bfloat16 [32, 1024, 4096], P('ep', 'tp'), may hold values from -0.09375 to 0.09375
- up_weight: bfloat16 [32, 1024, 4096], P('ep', 'tp'), may hold values from -0.09375 to 0.09375
- down_weight: bfloat16 [32, 1024, 4096], P('ep', None, 'tp'), may hold values from -0.1875 to 0.1875
Outputs:
- mixer_out: bfloat16 [16384, 4096], P('ep', 'tp')
- expert_out: bfloat16 [8192, 4096], P('ep', 'tp')
Inputs may be any that keep to these rules, and one draw needn't show every extreme that they name: `routes`: each row names 2 different experts. In the rows of one device no expert is named by more than 32 rows, and in the rows of some device an expert is named by exactly 32 rows.
All inputs are finite; a program needn't handle non-finite values.
Results may differ from a plain program's by a relative error of at most 0.0057.
Values may be sent and summed in bfloat16 or wider, within the bound.
A program may use at most 128 MiB of HBM per device.

v0:
```python
import functools

import jax
import jax.numpy as jnp
from jax import lax
from jax.experimental import pallas as pl
from jax.experimental.pallas import tpu as pltpu
from jax.sharding import PartitionSpec as P

EPSILON = 1e-06
LOG_FLOOR = -1e30
F32 = jnp.float32
BF16 = jnp.bfloat16
GROUPS = 4
PAD = 16


def flip(index, bits):
    place = 1
    while place <= bits:
        if bits & place:
            index = index + place * (1 - 2 * ((index // place) % 2))
        place *= 2
    return index


def dot(left, right, contract=((1,), (0,))):
    return lax.dot_general(left, right, (contract, ((), ())), preferred_element_type=F32)


def upright(row):
    size = row.shape[1]
    own = lax.broadcasted_iota(jnp.int32, (size, size), 0) == lax.broadcasted_iota(
        jnp.int32, (size, size), 1
    )
    return jnp.sum(jnp.where(own, row, jnp.zeros((), row.dtype)), axis=1, keepdims=True)


def kernel(
    ep,
    tp,
    head_count,
    model_width,
    x_ref,
    slot_row_ref,
    weight_ref,
    a_ref,
    cum_ref,
    gain_ref,
    q_hbm,
    k_hbm,
    v_hbm,
    og_hbm,
    wg_hbm,
    wu_hbm,
    wd_hbm,
    wm_hbm,
    mix_ref,
    exp_ref,
    q_ref,
    k_ref,
    v_ref,
    og_ref,
    wg_ref,
    wu_ref,
    wd_ref,
    wm_ref,
    slots,
    tok,
    hid,
    outb,
    ret,
    hm,
    local,
    st_in,
    st_out,
    load_sem,
    disp_send,
    disp_recv,
    tok_send,
    tok_recv,
    fwd_send,
    fwd_recv,
    hid_send,
    hid_recv,
    ret_send,
    ret_recv,
    head_send,
    head_recv,
    hfwd_send,
    hfwd_recv,
    st_send,
    st_recv,
):
    me = lax.axis_index("ep")
    mine = lax.axis_index("tp")
    cap = slots.shape[0] // ep
    span = slots.shape[0] // GROUPS
    per = ep // GROUPS
    width = x_ref.shape[1]
    length = q_ref.shape[0]
    qk = q_ref.shape[1] // head_count
    vw = v_ref.shape[1] // head_count
    units = wg_ref.shape[0]
    square = tp == 4

    loads = [
        pltpu.make_async_copy(source, target, load_sem.at[at])
        for at, (source, target) in enumerate(
            [
                (k_hbm, k_ref),
                (v_hbm, v_ref),
                (q_hbm, q_ref),
                (og_hbm, og_ref),
                (wg_hbm, wg_ref),
                (wu_hbm, wu_ref),
                (wd_hbm, wd_ref),
                (wm_hbm, wm_ref),
            ]
        )
    ]
    for load in loads:
        load.start()

    barrier = pltpu.get_barrier_semaphore()
    for i in range(1, ep):
        pl.semaphore_signal(barrier, inc=1, device_id={"ep": flip(me, i)})
    for j in range(1, tp):
        pl.semaphore_signal(barrier, inc=1, device_id={"tp": flip(mine, j)})

    tokens = x_ref.shape[0]

    def pick(group, carry):
        at = group * span
        rows = at + lax.broadcasted_iota(jnp.int32, (span, tokens), 0)
        hit = (rows == slot_row_ref[0:1, :]) | (rows == slot_row_ref[1:2, :])
        chosen = dot(hit.astype(F32).astype(BF16), x_ref[...]).astype(BF16)
        slots[pl.ds(pl.multiple_of(at, span), span), :] = chosen
        return carry

    lax.fori_loop(0, GROUPS, pick, 0)
    pl.semaphore_wait(barrier, ep - 1 + tp - 1)

    def dispatch(i):
        return pltpu.make_async_remote_copy(
            slots.at[pl.ds(i * cap, cap)],
            tok.at[0, pl.ds(i * cap, cap)],
            disp_send.at[i],
            disp_recv.at[i],
            device_id={"ep": flip(me, i)},
        )

    near = max(2, 2 * per)
    waits_for_chain = me % 2 == 1
    for i in range(1, ep):
        if i < near:
            dispatch(i).start()
        else:
            held = waits_for_chain & (flip(me, i) > me)

            @pl.when(jnp.logical_not(held))
            def _():
                dispatch(i).start()

    tok[0, 0:cap, :] = slots[0:cap, :]

    def spread(group, j):
        return pltpu.make_async_remote_copy(
            tok.at[0, pl.ds(group * span, span)],
            tok.at[j, pl.ds(group * span, span)],
            tok_send.at[group, j],
            tok_recv.at[group, j],
            device_id={"tp": flip(mine, j)},
        )

    half = span // 2

    def onward(group, j):
        part = pl.ds(group * span + (j - 1) * half, half)
        return pltpu.make_async_remote_copy(
            tok.at[j, part],
            tok.at[3, part],
            fwd_send.at[group, j],
            fwd_recv.at[group, j],
            device_id={"tp": flip(mine, 3 - j)},
        )

    direct = (1, 2) if square else tuple(range(1, tp))

    def send_group(group):
        for i in range(max(1, group * per), (group + 1) * per):
            dispatch(i).wait_recv()
        for j in direct:
            spread(group, j).start()

    def relay_group(group):
        if square:
            for j in (1, 2):
                spread(group, j).wait_recv()
                onward(group, j).start()

    def collect_group(group):
        if square:
            for j in (1, 2):
                onward(group, j).wait_recv()
        else:
            for j in direct:
                spread(group, j).wait_recv()

    send_group(0)

    loads[0].wait()
    loads[1].wait()

    def summarise(h, carry):
        keys = k_ref[:, pl.ds(pl.multiple_of(h * qk, qk), qk)]
        values = v_ref[:, pl.ds(pl.multiple_of(h * vw, vw), vw)]
        log_in = a_ref[pl.ds(h, 1), :]
        top = jnp.max(log_in, axis=1, keepdims=True)
        weighted = keys.astype(F32) * jnp.exp(upright(log_in) - top)
        local[h, 0:qk, :] = dot(weighted.astype(BF16), values, ((0,), (0,)))
        normal = jnp.sum(weighted, axis=0, keepdims=True)
        local[h, qk : qk + 8, 0:qk] = jnp.broadcast_to(normal, (8, qk))
        decay = cum_ref[pl.ds(h, 1), :][:, length - 1 : length]
        local[h, qk + 8 : qk + 16, :] = jnp.broadcast_to(top + decay, (8, vw))
        return carry

    lax.fori_loop(0, head_count, summarise, 0)

    @pl.when(me >= ep // 2)
    def _():
        send_group(1)
        relay_group(0)

    def chain(h):
        return pltpu.make_async_remote_copy(
            st_out.at[h],
            st_in.at[h],
            st_send.at[h],
            st_recv.at[h],
            device_id={"ep": me + 1},
        )

    @pl.when(me == 0)
    def _():
        st_in[:, 0 : qk + 8, :] = jnp.zeros((head_count, qk + 8, vw), F32)
        st_in[:, qk + 8 : qk + 16, :] = jnp.full((head_count, 8, vw), LOG_FLOOR, F32)

    for h in range(head_count):

        @pl.when(me > 0)
        def _():
            chain(h).wait_recv()

        decay = cum_ref[h : h + 1, length - 1 : length]
        carried_max = st_in[h, qk + 8 : qk + 9, :] + decay
        own_max = local[h, qk + 8 : qk + 9, :]
        new_max = jnp.maximum(carried_max, own_max)
        keep = jnp.exp(carried_max - new_max)
        add = jnp.exp(own_max - new_max)
        st_out[h, 0:qk, :] = keep * st_in[h, 0:qk, :] + add * local[h, 0:qk, :]
        st_out[h, qk : qk + 8, 0:qk] = (
            keep[:, 0:qk] * st_in[h, qk : qk + 8, 0:qk]
            + add[:, 0:qk] * local[h, qk : qk + 8, 0:qk]
        )
        st_out[h, qk : qk + 8, qk:vw] = jnp.zeros((8, vw - qk), F32)
        st_out[h, qk + 8 : qk + 16, :] = jnp.broadcast_to(new_max, (8, vw))

        @pl.when(me < ep - 1)
        def _():
            chain(h).start()

    for i in range(near, ep):
        held = waits_for_chain & (flip(me, i) > me)

        @pl.when(held)
        def _():
            dispatch(i).start()

    @pl.when(me < ep // 2)
    def _():
        send_group(1)
        relay_group(0)

    loads[2].wait()
    loads[3].wait()

    def heads(h, carry):
        columns = pl.ds(pl.multiple_of(h * vw, vw), vw)
        queries = q_ref[:, pl.ds(pl.multiple_of(h * qk, qk), qk)]
        keys = k_ref[:, pl.ds(pl.multiple_of(h * qk, qk), qk)]
        scale = qk**-0.5
        causal = lax.broadcasted_iota(jnp.int32, (length, length), 1) <= lax.broadcasted_iota(
            jnp.int32, (length, length), 0
        )
        log_in = jnp.where(causal, a_ref[pl.ds(h, 1), :], -jnp.inf)
        prior_max = st_in[h, qk + 8 : qk + 9, 0:1]
        top = jnp.maximum(prior_max, jnp.max(log_in, axis=1, keepdims=True))
        scores = dot(queries, keys, ((1,), (1,))) * scale * jnp.exp(log_in - top)
        carried = jnp.exp(prior_max - top) * scale
        memory = st_in[h, 0:qk, :]
        high = memory.astype(BF16)
        low = (memory - high.astype(F32)).astype(BF16)
        numerator = carried * (dot(queries, high) + dot(queries, low)) + dot(
            scores.astype(BF16), v_ref[:, columns]
        )
        normal = st_in[h, qk : qk + 1, 0:qk]
        denominator = carried * jnp.sum(
            queries.astype(F32) * normal, axis=1, keepdims=True
        ) + jnp.sum(scores, axis=1, keepdims=True)
        floor = jnp.exp(-(upright(cum_ref[pl.ds(h, 1), :]) + top))
        value = numerator / jnp.maximum(jnp.abs(denominator), floor)
        value = value * lax.rsqrt(jnp.mean(value * value, axis=1, keepdims=True) + EPSILON)
        gate = jax.nn.sigmoid(og_ref[:, columns].astype(F32))
        hm[0, :, columns] = (value * gain_ref[:, columns] * gate).astype(BF16)
        return carry

    lax.fori_loop(0, head_count // 2, heads, 0)
    relay_group(1)
    send_group(2)
    lax.fori_loop(head_count // 2, head_count, heads, 0)

    loads[4].wait()
    loads[5].wait()

    def expand(group):
        rows = pl.ds(group * span, span)

        gate = jnp.zeros((span, units), F32)
        up = jnp.zeros((span, units), F32)
        squares = jnp.zeros((span, 1), F32)
        for j in range(tp):
            piece = tok[j, rows, :]
            columns = pl.ds(pl.multiple_of(flip(mine, j) * width, width), width)
            gate += dot(piece, wg_ref[:, columns], ((1,), (1,)))
            up += dot(piece, wu_ref[:, columns], ((1,), (1,)))
            wide = piece.astype(F32)
            squares += jnp.sum(wide * wide, axis=1, keepdims=True)
        inverse = lax.rsqrt(squares / model_width + EPSILON)
        hid[0, rows, :] = (jax.nn.silu(gate * inverse) * (up * inverse)).astype(BF16)

    def share(group, j):
        return pltpu.make_async_remote_copy(
            hid.at[0, pl.ds(group * span, span)],
            hid.at[j, pl.ds(group * span, span)],
            hid_send.at[group, j],
            hid_recv.at[group, j],
            device_id={"tp": flip(mine, j)},
        )

    def give_back(i):
        return pltpu.make_async_remote_copy(
            outb.at[pl.ds(i * cap, cap)],
            ret.at[pl.ds(i * cap, cap)],
            ret_send.at[i],
            ret_recv.at[i],
            device_id={"ep": flip(me, i)},
        )

    def contract(group):
        rows = pl.ds(group * span, span)
        for j in range(1, tp):
            share(group, j).wait_recv()
        total = jnp.zeros((span, width), F32)
        for j in range(tp):
            at = pl.ds(pl.multiple_of(flip(mine, j) * units, units), units)
            total += dot(hid[j, rows, :], wd_ref[at, :])
        outb[rows, :] = total.astype(BF16)
        for i in range(max(1, group * per), (group + 1) * per):
            give_back(i).start()

    tile = length // 2

    def head_spread(part, j):
        rows = pl.ds(part * tile, tile)
        return pltpu.make_async_remote_copy(
            hm.at[0, rows],
            hm.at[j, rows],
            head_send.at[part, j],
            head_recv.at[part, j],
            device_id={"tp": flip(mine, j)},
        )

    def head_onward(part, j):
        rows = pl.ds(part * tile + (j - 1) * (tile // 2), tile // 2)
        return pltpu.make_async_remote_copy(
            hm.at[j, rows],
            hm.at[3, rows],
            hfwd_send.at[part, j],
            hfwd_recv.at[part, j],
            device_id={"tp": flip(mine, 3 - j)},
        )

    def expand_and_share(group):
        collect_group(group)
        expand(group)
        for j in range(1, tp):
            share(group, j).start()

    loads[6].wait()
    for group in range(GROUPS):
        if group > 1:
            if group + 1 < GROUPS:
                relay_group(group + 1)
        expand_and_share(group)
        if group == 0:
            for later in range(3, GROUPS):
                send_group(later)
            relay_group(2)
        elif group < GROUPS - 1:
            contract(group - 1)
    for part in range(2):
        for j in direct:
            head_spread(part, j).start()
    contract(GROUPS - 2)
    contract(GROUPS - 1)
    ret[0:cap, :] = outb[0:cap, :]

    loads[7].wait()
    if square:
        for part in range(2):
            for j in (1, 2):
                head_spread(part, j).wait_recv()
                head_onward(part, j).start()

    def mix(part):
        rows = pl.ds(part * tile, tile)
        for j in range(1, tp):
            if not square:
                head_spread(part, j).wait_recv()
            elif j < 3:
                head_onward(part, j).wait_recv()
        total = jnp.zeros((tile, width), F32)
        for j in range(tp):
            inputs = pl.ds(pl.multiple_of(flip(mine, j) * width, width), width)
            total += dot(hm[j, rows, :], wm_ref[inputs, :])
        mix_ref[rows, :] = total.astype(BF16)

    mix(0)

    for i in range(1, ep):
        give_back(i).wait_recv()
    places = lax.broadcasted_iota(jnp.int32, (slots.shape[0], tokens), 0)
    total = jnp.zeros((tokens, width), F32)
    for route in range(weight_ref.shape[0]):
        hit = places == slot_row_ref[route : route + 1, :]
        picked = dot(hit.astype(F32).astype(BF16), ret[...], ((0,), (0,)))
        total += picked * upright(weight_ref[route : route + 1, :])
    exp_ref[...] = total.astype(BF16)

    mix(1)

    for i in range(1, ep):
        dispatch(i).wait_send()
        give_back(i).wait_send()
    for group in range(GROUPS):
        for j in direct:
            spread(group, j).wait_send()
        for j in range(1, tp):
            share(group, j).wait_send()
        if square:
            for j in (1, 2):
                onward(group, j).wait_send()
    for part in range(2):
        for j in direct:
            head_spread(part, j).wait_send()
        if square:
            for j in (1, 2):
                head_onward(part, j).wait_send()
    for h in range(head_count):

        @pl.when(me < ep - 1)
        def _():
            chain(h).wait_send()


def body(
    query_rows,
    key_rows,
    value_rows,
    in_gate,
    forget_gate,
    out_gate,
    head_gain,
    mix_weight,
    expert_input,
    routes,
    route_weight,
    gate_weight,
    up_weight,
    down_weight,
):
    ep, tp = lax.axis_size("ep"), lax.axis_size("tp")
    head_count, length = in_gate.shape
    token_count, fanout = routes.shape
    width = expert_input.shape[1]
    units = gate_weight.shape[1]
    capacity = 2 * token_count * fanout // ep
    slot_count = ep * capacity
    qk = query_rows.shape[1] // head_count
    vw = value_rows.shape[1] // head_count

    earlier = jnp.tril(jnp.ones((length, length), F32))
    cumulative = jnp.einsum(
        "hs,ts->ht", jax.nn.log_sigmoid(forget_gate), earlier, precision=lax.Precision.HIGHEST
    )
    shifted = in_gate - cumulative

    me = lax.axis_index("ep")
    turned = routes ^ me
    experts = jnp.arange(ep, dtype=jnp.int32)
    named = turned[:, :, None] == experts
    any_named = jnp.any(named, axis=1)
    before = jnp.dot(
        jnp.tril(jnp.ones((token_count, token_count), BF16), -1),
        any_named.astype(BF16),
        preferred_element_type=F32,
    ).astype(jnp.int32)
    places = experts * capacity + before
    slot_row = jnp.sum(jnp.where(named, places[:, None, :], 0), axis=2).T

    vmem = pl.BlockSpec(memory_space=pltpu.VMEM)
    anywhere = pl.BlockSpec(memory_space=pl.ANY)
    dma = pltpu.SemaphoreType.DMA
    gate_local, up_local, down_local = gate_weight[0], up_weight[0], down_weight[0]
    big = (query_rows, key_rows, value_rows, out_gate, gate_local, up_local, down_local, mix_weight)
    state = (head_count, qk + PAD, vw)
    return pl.pallas_call(
        functools.partial(kernel, ep, tp, head_count, mix_weight.shape[0]),
        out_shape=(
            jax.ShapeDtypeStruct((length, width), BF16),
            jax.ShapeDtypeStruct((token_count, width), BF16),
        ),
        in_specs=[vmem] * 6 + [anywhere] * 8,
        out_specs=(vmem, vmem),
        scratch_shapes=[pltpu.VMEM(array.shape, array.dtype) for array in big]
        + [
            pltpu.VMEM((slot_count, width), BF16),
            pltpu.VMEM((tp, slot_count, width), BF16),
            pltpu.VMEM((tp, slot_count, units), BF16),
            pltpu.VMEM((slot_count, width), BF16),
            pltpu.VMEM((slot_count, width), BF16),
            pltpu.VMEM((tp, length, width), BF16),
            pltpu.VMEM(state, F32),
            pltpu.VMEM(state, F32),
            pltpu.VMEM(state, F32),
            dma((8,)),
            dma((ep,)),
            dma((ep,)),
            dma((GROUPS, tp)),
            dma((GROUPS, tp)),
            dma((GROUPS, 4)),
            dma((GROUPS, 4)),
            dma((GROUPS, tp)),
            dma((GROUPS, tp)),
            dma((ep,)),
            dma((ep,)),
            dma((2, tp)),
            dma((2, tp)),
            dma((2, 4)),
            dma((2, 4)),
            dma((head_count,)),
            dma((head_count,)),
        ],
        compiler_params=pltpu.CompilerParams(
            collective_id=0, has_side_effects=True, vmem_limit_bytes=64000 * 1024
        ),
    )(
        expert_input,
        slot_row,
        route_weight.T,
        shifted,
        cumulative,
        head_gain[None, :],
        *big,
    )


def solution(mesh):
    in_specs = (
        P("ep", "tp"),
        P("ep", "tp"),
        P("ep", "tp"),
        P("tp", "ep"),
        P("tp", "ep"),
        P("ep", "tp"),
        P("tp"),
        P(None, "tp"),
        P("ep", "tp"),
        P("ep", None),
        P("ep", None),
        P("ep", "tp", None),
        P("ep", "tp", None),
        P("ep", None, "tp"),
    )
    out_specs = (P("ep", "tp"), P("ep", "tp"))
    return jax.shard_map(body, mesh=mesh, in_specs=in_specs, out_specs=out_specs, check_vma=False)
```

profile of v0, /device:TPU:487, one launch (start us, length us, event | category | flops | bytes accessed | tf_op | source)
XLA Modules:
  0.0 288.2 jit_solution(17424988315989230632)
XLA Ops:
  0.7 0.7 broadcast_xor_fusion
  1.3 1.9 fusion.20
  3.3 0.2 fusion
  3.5 0.6 select_reduce_fusion
  4.2 280.8 %shard_map.149 = (bf16[512,256]{1,0:T(8,128)(2,1)}, bf16[256,256]{1,0:T(8,128)(2,1)}) custom-call(bf16[256,256]{1,0:T(8,128)(2,1)} %x_ref.1, s32[2,256]{1,0:T(2,128)} %bitcast.17, f32[2,256]{1,0:T(2,128)} %bitcast.18, f32[1,512]{1,0:T(1,128)} %get-tuple-element.2.a_ref, f32[1,512]{1,0:T(1,128)} %get-tuple-element.3.cum_ref, f32[1,256]{1,0:T(1,128)} %bitcast.19, ...), custom_call_target="tpu_custom_call" | custom-call | tf_op jit(solution)/shard_map/pallas_call | solution.py:528
  285.0 1.7 copy.20
  286.7 1.6 copy.21
  (3 shorter events, 0.0 us)
where the time goes:
time: 288 us
  Pallas kernels  281 us (98%)
  local copies, waits for them, and re-layouts  3.24 us (1%)
    pallas_call x1, Pallas kernels, body(): pl.pallas_call(functools.partial(kernel, ep, tp, head_count, mix_weight.s...  281 us

commit v1 on v0

v1 whole, which is shorter than its diff:
```python
import functools

import jax
import jax.numpy as jnp
from jax import lax
from jax.experimental import pallas as pl
from jax.experimental.pallas import tpu as pltpu
from jax.sharding import PartitionSpec as P

EPSILON = 1e-06
LOG_FLOOR = -1e30
F32 = jnp.float32
BF16 = jnp.bfloat16
GROUPS = 4
SIDE = 4
PARTS = 2
CHUNKS = 4
HEAD = 8
HOLD = 4


def flip(index, bits):
    place = 1
    while place <= bits:
        if bits & place:
            index = index + place * (1 - 2 * ((index // place) % 2))
        place *= 2
    return index


def dot(left, right, contract=((1,), (0,))):
    return lax.dot_general(left, right, (contract, ((), ())), preferred_element_type=F32)


def own_mask(size):
    return lax.broadcasted_iota(jnp.int32, (size, size), 0) == lax.broadcasted_iota(
        jnp.int32, (size, size), 1
    )


def upright(row):
    size = row.shape[1]
    return jnp.sum(jnp.where(own_mask(size), row, 0.0), axis=1, keepdims=True)


def flat(column):
    size = column.shape[0]
    return jnp.sum(jnp.where(own_mask(size), column, 0.0), axis=0, keepdims=True)


def kernel(
    ep,
    tp,
    model_width,
    x_ref,
    slot_row_ref,
    weight_ref,
    a_ref,
    cum_ref,
    gain_ref,
    q_hbm,
    k_hbm,
    v_hbm,
    og_hbm,
    wg_hbm,
    wu_hbm,
    wd_hbm,
    wm_hbm,
    mix_ref,
    exp_ref,
    q_ref,
    k_ref,
    v_ref,
    og_ref,
    wd_ref,
    wm_ref,
    wm_turned,
    w1,
    w2,
    slots,
    tok,
    part_own,
    part_out,
    part_in,
    sq_out,
    sq_in,
    hid,
    outb,
    ret,
    hm,
    num_ref,
    den_ref,
    top_ref,
    loc,
    pair_in,
    both,
    st_in,
    st_out,
    prior,
    load_sem,
    own_sem,
    deal_send,
    deal_recv,
    disp_send,
    disp_recv,
    tok_send,
    tok_recv,
    part_send,
    part_recv,
    sq_send,
    sq_recv,
    hid_send,
    hid_recv,
    ret_send,
    ret_recv,
    head_send,
    head_recv,
    pair_send,
    pair_recv,
    down_send,
    down_recv,
    st_send,
    st_recv,
):
    me = lax.axis_index("ep")
    mine = lax.axis_index("tp")
    row, column = mine // SIDE, mine % SIDE
    chip, core = me // 2, me % 2
    chips = ep // 2
    cap = slots.shape[0] // ep
    span = slots.shape[0] // GROUPS
    half_span = span // 2
    per = ep // GROUPS
    width = x_ref.shape[1]
    tokens = x_ref.shape[0]
    length, qk = q_ref.shape
    vw = v_ref.shape[1]
    units = wg_hbm.shape[0]
    wide = SIDE * width
    last = chips - 1

    loads = [
        pltpu.make_async_copy(source, target, load_sem.at[at])
        for at, (source, target) in enumerate(
            [
                (k_hbm, k_ref),
                (v_hbm, v_ref),
                (q_hbm, q_ref),
                (og_hbm, og_ref),
                (wd_hbm, wd_ref),
                (wm_hbm, wm_ref),
            ]
        )
    ]
    for load in loads:
        load.start()

    def piece(source, j, k):
        start = pl.multiple_of((flip(row, k) * SIDE + flip(column, j)) * width, width)
        return source.at[:, pl.ds(start, width)]

    def slot_of(j, which, k):
        return w1.at[pl.ds((2 * j + which) * units, units), pl.ds(k * width, width)]

    own_pieces = [
        pltpu.make_async_copy(
            piece(source, 0, k), slot_of(0, which, k), own_sem.at[which * SIDE + k]
        )
        for which, source in enumerate((wg_hbm, wu_hbm))
        for k in range(SIDE)
    ]
    for load in own_pieces:
        load.start()

    def deal(j, which, k):
        at = (j - 1) * 2 * SIDE + which * SIDE + k
        return pltpu.make_async_remote_copy(
            piece(wu_hbm if which else wg_hbm, j, k),
            slot_of(j, which, k),
            deal_send.at[at],
            deal_recv.at[at],
            device_id={"tp": flip(mine, j)},
        )

    dealt = [(j, which, k) for j in range(1, SIDE) for which in range(2) for k in range(SIDE)]

    barrier = pltpu.get_barrier_semaphore()
    for i in range(1, ep):
        pl.semaphore_signal(barrier, inc=1, device_id={"ep": flip(me, i)})
    for j in range(1, tp):
        pl.semaphore_signal(barrier, inc=1, device_id={"tp": flip(mine, j)})

    def pick(group, carry):
        at = group * span
        rows = at + lax.broadcasted_iota(jnp.int32, (span, tokens), 0)
        hit = (rows == slot_row_ref[0:1, :]) | (rows == slot_row_ref[1:2, :])
        chosen = dot(hit.astype(F32).astype(BF16), x_ref[...]).astype(BF16)
        slots[pl.ds(pl.multiple_of(at, span), span), :] = chosen
        return carry

    lax.fori_loop(0, GROUPS, pick, 0)

    loads[0].wait()
    loads[1].wait()
    decay = cum_ref[0:1, length - 1 : length]
    log_in = a_ref[0:1, :]
    local_top = jnp.max(log_in, axis=1, keepdims=True)
    weighted = k_ref[...].astype(F32) * jnp.exp(upright(log_in) - local_top)
    loc[HEAD : HEAD + qk, :] = dot(weighted.astype(BF16), v_ref[...], ((0,), (0,)))
    loc[0:HEAD, 0:qk] = jnp.broadcast_to(jnp.sum(weighted, axis=0, keepdims=True), (HEAD, qk))
    loc[0:HEAD, qk:vw] = jnp.broadcast_to(local_top + decay, (HEAD, vw - qk))
    loc[HEAD + qk :, :] = jnp.broadcast_to(decay, (8, vw))

    @pl.when(chip == 0)
    def _():
        st_in[0:HEAD, 0:qk] = jnp.zeros((HEAD, qk), F32)
        st_in[0:HEAD, qk:vw] = jnp.full((HEAD, vw - qk), LOG_FLOOR, F32)
        st_in[HEAD:, :] = jnp.zeros((qk, vw), F32)

    pl.semaphore_wait(barrier, ep - 1 + tp - 1)

    pair = pltpu.make_async_remote_copy(
        loc, pair_in, pair_send.at[0], pair_recv.at[0], device_id={"ep": flip(me, 1)}
    )

    @pl.when(core == 0)
    def _():
        pair.start()

    def dispatch(i):
        return pltpu.make_async_remote_copy(
            slots.at[pl.ds(i * cap, cap)],
            tok.at[pl.ds(i * cap, cap), pl.ds(0, width)],
            disp_send.at[i],
            disp_recv.at[i],
            device_id={"ep": flip(me, i)},
        )

    def held(i):
        ahead = (flip(chip, i // 2) - chip + chips) % chips
        return (core == 1) & (chip < HOLD) & (ahead > 0) & (ahead <= chips // 2)

    for i in range(1, ep):

        @pl.when(jnp.logical_not(held(i)))
        def _():
            dispatch(i).start()

    tok[0:cap, 0:width] = slots[0:cap, :]
    for each in dealt:
        deal(*each).start()

    def gates(first_max, second_max):
        top = jnp.maximum(first_max, second_max)
        return top, jnp.exp(first_max - top), jnp.exp(second_max - top)

    def merge(target, lower, upper, keep, add, top):
        if lower == 0:
            first, second = target[1], target[2]
            target[0][0:HEAD, 0:qk] = keep * first[0:HEAD, 0:qk] + add * second[0:HEAD, 0:qk]
            target[0][0:HEAD, qk:vw] = jnp.broadcast_to(top, (HEAD, vw - qk))
            lower = HEAD
        target[0][lower:upper, :] = (
            keep * target[1][lower:upper, :] + add * target[2][lower:upper, :]
        )

    edges = [0] + [HEAD + (at + 1) * (qk // CHUNKS) for at in range(CHUNKS)]

    def chain(at):
        rows = pl.ds(edges[at], edges[at + 1] - edges[at])
        return pltpu.make_async_remote_copy(
            st_out.at[rows],
            st_in.at[rows],
            st_send.at[at],
            st_recv.at[at],
            device_id={"ep": me + 2},
        )

    def down(at):
        rows = pl.ds(edges[at], edges[at + 1] - edges[at])
        return pltpu.make_async_remote_copy(
            st_in.at[rows],
            st_in.at[rows],
            down_send.at[at],
            down_recv.at[at],
            device_id={"ep": flip(me, 1)},
        )

    @pl.when(core == 1)
    def _():
        pair.wait_recv()
        top, keep, add = gates(
            pair_in[0:1, qk : qk + 1] + decay,
            loc[0:1, qk : qk + 1],
        )
        merge((both, pair_in, loc), 0, HEAD + qk, keep, add, top)

    def chain_step():
        both_decay = pair_in[HEAD + qk : HEAD + qk + 1, 0:1] + decay
        keep = add = top = None
        for at in range(CHUNKS):

            @pl.when(chip > 0)
            def _():
                chain(at).wait_recv()
                down(at).start()

            if at == 0:
                top, keep, add = gates(
                    st_in[0:1, qk : qk + 1] + both_decay, both[0:1, qk : qk + 1]
                )

            merge((st_out, st_in, both), edges[at], edges[at + 1], keep, add, top)

            @pl.when(chip < last)
            def _():
                chain(at).start()

    ticks = GROUPS + 7

    def chain_slot(tick):
        turn = jnp.maximum(chip * 5 // 8 - 1, -1)

        @pl.when((core == 1) & (turn == tick))
        def _():
            chain_step()

    chain_slot(-1)

    loads[2].wait()
    tile = length // 4
    scale = qk**-0.5
    for at in range(4):
        rows = pl.ds(at * tile, tile)
        seen = (at + 1) * tile
        causal = lax.broadcasted_iota(jnp.int32, (tile, seen), 1) <= at * tile + (
            lax.broadcasted_iota(jnp.int32, (tile, seen), 0)
        )
        log_seen = jnp.where(causal, a_ref[0:1, 0:seen], -jnp.inf)
        top = jnp.max(log_seen, axis=1, keepdims=True)
        scores = dot(q_ref[rows, :], k_ref[0:seen, :], ((1,), (1,))) * scale
        scores = scores * jnp.exp(log_seen - top)
        num_ref[rows, :] = dot(scores.astype(BF16), v_ref[0:seen, :])
        den_ref[rows, :] = jnp.broadcast_to(jnp.sum(scores, axis=1, keepdims=True), (tile, 128))
        top_ref[rows, :] = jnp.broadcast_to(top, (tile, 128))

    loads[4].wait()
    nothing = jnp.zeros((units, width), BF16)
    for turned in range(2):
        for at in range(tp):
            unit = (at % SIDE) * SIDE + at // SIDE if turned else at
            block = wd_ref[unit * units : (unit + 1) * units, :]
            first = at * 2 * units
            w2[turned, first : first + units, 0:width] = block
            w2[turned, first : first + units, width : 2 * width] = nothing
            w2[turned, first + units : first + 2 * units, 0:width] = nothing
            w2[turned, first + units : first + 2 * units, width : 2 * width] = block
    loads[5].wait()

    def turn_block(at, carry):
        source = pl.multiple_of(((at % SIDE) * SIDE + at // SIDE) * width, width)
        target = pl.multiple_of(at * width, width)
        wm_turned[pl.ds(target, width), :] = wm_ref[pl.ds(source, width), :]
        return carry

    lax.fori_loop(0, tp, turn_block, 0)


    def spread(group, k):
        rows = pl.ds(group * span, span)
        return pltpu.make_async_remote_copy(
            tok.at[rows, pl.ds(0, width)],
            tok.at[rows, pl.ds(k * width, width)],
            tok_send.at[group, k],
            tok_recv.at[group, k],
            device_id={"tp": flip(mine, SIDE * k)},
        )

    def onward(group, k):
        rows = pl.ds(group * span + (k // 2) * half_span, half_span)
        return pltpu.make_async_remote_copy(
            tok.at[rows, pl.ds(k * width, width)],
            tok.at[rows, pl.ds(2 * width, width)],
            tok_send.at[group, 4 + k],
            tok_recv.at[group, 4 + k],
            device_id={"tp": flip(mine, SIDE * (SIDE - k))},
        )

    def send_partial(group, j):
        rows = pl.ds(group * span, span)
        return pltpu.make_async_remote_copy(
            part_out.at[j, rows],
            part_in.at[j, rows],
            part_send.at[group, j],
            part_recv.at[group, j],
            device_id={"tp": flip(mine, j)},
        )

    def send_squares(group, j):
        return pltpu.make_async_remote_copy(
            sq_out.at[group],
            sq_in.at[group, j],
            sq_send.at[group, j],
            sq_recv.at[group, j],
            device_id={"tp": flip(mine, j)},
        )


    def gather_copies(buffer, first_row, rows, wide_block, x_first, send, recv):
        inner, outer = (column, row) if x_first else (row, column)
        inner_bits, outer_bits = (1, SIDE) if x_first else (SIDE, 1)
        base = outer * SIDE * wide_block
        half = rows // 2

        def cut(part, block, count):
            begin, extent = (first_row, rows) if part is None else (first_row + part * half, half)
            return buffer.at[
                pl.ds(begin, extent),
                pl.ds(pl.multiple_of(base + block * wide_block, wide_block), count * wide_block),
            ]

        def outer_cut(part, bits):
            begin, extent = (first_row, rows) if part is None else (first_row + part * half, half)
            start = pl.multiple_of(flip(outer, bits) * SIDE * wide_block, SIDE * wide_block)
            return buffer.at[pl.ds(begin, extent), pl.ds(start, SIDE * wide_block)]

        def remote(piece_of, at, bits):
            return pltpu.make_async_remote_copy(
                piece_of, piece_of, send.at[at], recv.at[at], device_id={"tp": flip(mine, bits)}
            )

        def inner_send(k):
            return remote(cut(None, inner, 1), k // 2, k * inner_bits)

        def inner_relay(k):
            return remote(
                cut(k // 2, flip(inner, k), 1), 2 + k // 2, (SIDE - k) * inner_bits
            )

        def outer_send(k):
            return remote(outer_cut(None, 0), 4 + k // 2, k * outer_bits)

        def outer_relay(k):
            return remote(outer_cut(k // 2, k), 6 + k // 2, (SIDE - k) * outer_bits)

        return [[make(k) for k in (1, 3)] for make in (inner_send, inner_relay, outer_send, outer_relay)]

    def gather_step(copies, step):
        if step > 0:
            for copy in copies[step - 1]:
                copy.wait_recv()
        if step < 4:
            for copy in copies[step]:
                copy.start()

    hid_copies = [
        gather_copies(
            hid,
            group * half_span,
            half_span,
            2 * units,
            group % 2 == 0,
            hid_send.at[group],
            hid_recv.at[group],
        )
        for group in range(GROUPS)
    ]

    def give_back(i):
        return pltpu.make_async_remote_copy(
            outb.at[pl.ds(i * cap, cap)],
            ret.at[pl.ds(i * cap, cap)],
            ret_send.at[i],
            ret_recv.at[i],
            device_id={"ep": flip(me, i)},
        )

    def stage(group, step):
        rows = pl.ds(group * span, span)
        packed = pl.ds(group * half_span, half_span)
        if step == 0:
            for i in range(max(1, group * per), (group + 1) * per):
                dispatch(i).wait_recv()
            for k in (1, 3):
                spread(group, k).start()
        elif step == 1:
            for k in (1, 3):
                spread(group, k).wait_recv()
                onward(group, k).start()
        elif step == 2:
            if group == 0:
                for load in own_pieces:
                    load.wait()
                for each in dealt:
                    deal(*each).wait_recv()
            for k in (1, 3):
                onward(group, k).wait_recv()
            piece_of = tok[rows, :]
            partial = dot(piece_of, w1[...], ((1,), (1,)))
            part_own[rows, :] = partial[:, 0 : 2 * units]
            for j in range(1, SIDE):
                part_out[j, rows, :] = partial[:, j * 2 * units : (j + 1) * 2 * units].astype(BF16)
            for j in range(1, SIDE):
                send_partial(group, j).start()
            full = piece_of.astype(F32)
            squares = flat(jnp.sum(full * full, axis=1, keepdims=True))
            sq_out[group] = jnp.broadcast_to(squares, (8, span))
            for j in range(1, SIDE):
                send_squares(group, j).start()
        elif step == 3:
            squares = sq_out[group][0:1, :]
            for j in range(1, SIDE):
                send_squares(group, j).wait_recv()
                squares = squares + sq_in[group, j][0:1, :]
            inverse = upright(lax.rsqrt(squares / model_width + EPSILON))
            total = part_own[rows, :]
            for j in range(1, SIDE):
                send_partial(group, j).wait_recv()
                total = total + part_in[j, rows, :].astype(F32)
            total = total * inverse
            hidden = jax.nn.silu(total) * pltpu.roll(total, units, 1)
            turned = pltpu.roll(hidden, units, 1)
            lanes = lax.broadcasted_iota(jnp.int32, (half_span, 2 * units), 1)
            both_rows = jnp.where(lanes < units, hidden[0:half_span, :], turned[half_span:span, :])
            place = mine if group % 2 == 0 else column * SIDE + row
            columns = pl.ds(pl.multiple_of(place * 2 * units, 2 * units), 2 * units)
            hid[packed, columns] = both_rows.astype(BF16)
            gather_step(hid_copies[group], 0)
        elif step < 7:
            gather_step(hid_copies[group], step - 3)
        else:
            gather_step(hid_copies[group], 4)
            total = dot(hid[packed, :], w2[group % 2])
            outb[pl.ds(group * span, half_span), :] = total[:, 0:width].astype(BF16)
            outb[pl.ds(group * span + half_span, half_span), :] = total[:, width:].astype(BF16)
            for i in range(max(1, group * per), (group + 1) * per):
                give_back(i).start()

    for tick in range(ticks):
        if tick < 9:
            chain_slot(tick)
        if tick == 0:
            for i in range(1, ep):

                @pl.when(held(i))
                def _():
                    dispatch(i).start()

        for group in range(GROUPS):
            if 0 <= tick - group < 8:
                stage(group, tick - group)
    ret[0:cap, :] = outb[0:cap, :]


    @pl.when((core == 0) & (chip > 0))
    def _():
        for at in range(CHUNKS):
            down(at).wait_recv()

    @pl.when(core == 0)
    def _():
        prior[...] = st_in[...]

    @pl.when(core == 1)
    def _():
        other_decay = pair_in[HEAD + qk : HEAD + qk + 1, 0:1]
        top, keep, add = gates(
            st_in[0:1, qk : qk + 1] + other_decay, pair_in[0:1, qk : qk + 1]
        )
        merge((prior, st_in, pair_in), 0, HEAD + qk, keep, add, top)

    loads[3].wait()
    part_rows = length // (2 * PARTS)
    head_copies = [
        gather_copies(
            hm.at[at // PARTS],
            (at % PARTS) * part_rows,
            part_rows,
            width,
            at // PARTS == 0,
            head_send.at[at],
            head_recv.at[at],
        )
        for at in range(2 * PARTS)
    ]
    prior_max = prior[0:1, qk : qk + 1]
    normal = prior[0:1, 0:qk]
    memory = prior[HEAD:, :]
    high = memory.astype(BF16)
    low = (memory - high.astype(F32)).astype(BF16)
    for order in range(2 * PARTS):
        at = order // 2 + (order % 2) * PARTS
        rows = pl.ds(at * part_rows, part_rows)
        queries = q_ref[rows, :]
        own_top = top_ref[rows, 0:1]
        top = jnp.maximum(prior_max, own_top)
        again = jnp.exp(own_top - top)
        carried = jnp.exp(prior_max - top) * scale
        numerator = carried * (dot(queries, high) + dot(queries, low)) + again * num_ref[rows, :]
        denominator = (
            carried * jnp.sum(queries.astype(F32) * normal, axis=1, keepdims=True)
            + again * den_ref[rows, 0:1]
        )
        cumulative = upright(cum_ref[0:1, at * part_rows : (at + 1) * part_rows])
        floor = jnp.exp(-(cumulative + top))
        value = numerator / jnp.maximum(jnp.abs(denominator), floor)
        value = value * lax.rsqrt(jnp.mean(value * value, axis=1, keepdims=True) + EPSILON)
        gate = jax.nn.sigmoid(og_ref[rows, :].astype(F32))
        place = mine if at < PARTS else column * SIDE + row
        hm[
            at // PARTS,
            pl.ds((at % PARTS) * part_rows, part_rows),
            pl.ds(pl.multiple_of(place * width, width), width),
        ] = (value * gain_ref[...] * gate).astype(BF16)
        gather_step(head_copies[at], 0)

    for step in range(1, 5):
        for order in range(2 * PARTS):
            at = order // 2 + (order % 2) * PARTS
            gather_step(head_copies[at], step)
            if step == 4:
                inputs = hm[at // PARTS, pl.ds((at % PARTS) * part_rows, part_rows), :]
                weights = wm_ref if at < PARTS else wm_turned
                mix_ref[pl.ds(at * part_rows, part_rows), :] = dot(inputs, weights[...]).astype(BF16)

    total = jnp.zeros((tokens, width), F32)
    places = lax.broadcasted_iota(jnp.int32, (span, tokens), 0)
    weights = [upright(weight_ref[route : route + 1, :]) for route in range(weight_ref.shape[0])]
    for group in range(GROUPS):
        for i in range(max(1, group * per), (group + 1) * per):
            give_back(i).wait_recv()
        rows = pl.ds(group * span, span)
        for route, weight in enumerate(weights):
            hit = places == slot_row_ref[route : route + 1, :] - group * span
            picked = dot(hit.astype(F32).astype(BF16), ret[rows, :], ((0,), (0,)))
            total += picked * weight
    exp_ref[...] = total.astype(BF16)

    for i in range(1, ep):
        dispatch(i).wait_send()
        give_back(i).wait_send()
    for each in dealt:
        deal(*each).wait_send()
    for group in range(GROUPS):
        for k in (1, 3):
            spread(group, k).wait_send()
            onward(group, k).wait_send()
        for j in range(1, SIDE):
            send_partial(group, j).wait_send()
            send_squares(group, j).wait_send()
    for copies in hid_copies + head_copies:
        for step in copies:
            for copy in step:
                copy.wait_send()

    @pl.when(core == 0)
    def _():
        pair.wait_send()

    for at in range(CHUNKS):

        @pl.when((core == 1) & (chip > 0))
        def _():
            down(at).wait_send()

        @pl.when((core == 1) & (chip < last))
        def _():
            chain(at).wait_send()


def body(
    query_rows,
    key_rows,
    value_rows,
    in_gate,
    forget_gate,
    out_gate,
    head_gain,
    mix_weight,
    expert_input,
    routes,
    route_weight,
    gate_weight,
    up_weight,
    down_weight,
):
    ep, tp = lax.axis_size("ep"), lax.axis_size("tp")
    length = in_gate.shape[1]
    token_count, fanout = routes.shape
    width = expert_input.shape[1]
    units = gate_weight.shape[1]
    capacity = 2 * token_count * fanout // ep
    slot_count = ep * capacity
    qk = query_rows.shape[1]
    vw = value_rows.shape[1]

    earlier = jnp.tril(jnp.ones((length, length), F32))
    cumulative = jnp.einsum(
        "hs,ts->ht", jax.nn.log_sigmoid(forget_gate), earlier, precision=lax.Precision.HIGHEST
    )
    shifted = in_gate - cumulative

    me = lax.axis_index("ep")
    turned = routes ^ me
    experts = jnp.arange(ep, dtype=jnp.int32)
    named = turned[:, :, None] == experts
    any_named = jnp.any(named, axis=1)
    before = jnp.dot(
        jnp.tril(jnp.ones((token_count, token_count), BF16), -1),
        any_named.astype(BF16),
        preferred_element_type=F32,
    ).astype(jnp.int32)
    places = experts * capacity + before
    slot_row = jnp.sum(jnp.where(named, places[:, None, :], 0), axis=2).T

    vmem = pl.BlockSpec(memory_space=pltpu.VMEM)
    anywhere = pl.BlockSpec(memory_space=pl.ANY)
    dma = pltpu.SemaphoreType.DMA
    gate_local, up_local, down_local = gate_weight[0], up_weight[0], down_weight[0]
    big = (query_rows, key_rows, value_rows, out_gate, gate_local, up_local, down_local, mix_weight)
    held = (query_rows, key_rows, value_rows, out_gate, down_local, mix_weight, mix_weight)
    deals = (SIDE - 1) * 2 * SIDE
    state = (HEAD + qk, vw)
    tall = (HEAD + qk + 8, vw)
    return pl.pallas_call(
        functools.partial(kernel, ep, tp, mix_weight.shape[0]),
        out_shape=(
            jax.ShapeDtypeStruct((length, width), BF16),
            jax.ShapeDtypeStruct((token_count, width), BF16),
        ),
        in_specs=[vmem] * 6 + [anywhere] * 8,
        out_specs=(vmem, vmem),
        scratch_shapes=[pltpu.VMEM(array.shape, array.dtype) for array in held]
        + [
            pltpu.VMEM((SIDE * 2 * units, SIDE * width), BF16),
            pltpu.VMEM((2, tp * 2 * units, 2 * width), BF16),
            pltpu.VMEM((slot_count, width), BF16),
            pltpu.VMEM((slot_count, SIDE * width), BF16),
            pltpu.VMEM((slot_count, 2 * units), F32),
            pltpu.VMEM((SIDE, slot_count, 2 * units), BF16),
            pltpu.VMEM((SIDE, slot_count, 2 * units), BF16),
            pltpu.VMEM((GROUPS, 8, slot_count // GROUPS), F32),
            pltpu.VMEM((GROUPS, SIDE, 8, slot_count // GROUPS), F32),
            pltpu.VMEM((slot_count // 2, tp * 2 * units), BF16),
            pltpu.VMEM((slot_count, width), BF16),
            pltpu.VMEM((slot_count, width), BF16),
            pltpu.VMEM((2, length // 2, tp * width), BF16),
            pltpu.VMEM((length, vw), F32),
            pltpu.VMEM((length, 128), F32),
            pltpu.VMEM((length, 128), F32),
            pltpu.VMEM(tall, F32),
            pltpu.VMEM(tall, F32),
            pltpu.VMEM(state, F32),
            pltpu.VMEM(state, F32),
            pltpu.VMEM(state, F32),
            pltpu.VMEM(state, F32),
            dma((6,)),
            dma((2 * SIDE,)),
            dma((deals,)),
            dma((deals,)),
            dma((ep,)),
            dma((ep,)),
            dma((GROUPS, 8)),
            dma((GROUPS, 8)),
            dma((GROUPS, SIDE)),
            dma((GROUPS, SIDE)),
            dma((GROUPS, SIDE)),
            dma((GROUPS, SIDE)),
            dma((GROUPS, 8)),
            dma((GROUPS, 8)),
            dma((ep,)),
            dma((ep,)),
            dma((2 * PARTS, 8)),
            dma((2 * PARTS, 8)),
            dma((1,)),
            dma((1,)),
            dma((CHUNKS,)),
            dma((CHUNKS,)),
            dma((CHUNKS,)),
            dma((CHUNKS,)),
        ],
        compiler_params=pltpu.CompilerParams(
            collective_id=0, has_side_effects=True, vmem_limit_bytes=64000 * 1024
        ),
    )(
        expert_input,
        slot_row,
        route_weight.T,
        shifted,
        cumulative,
        head_gain[None, :],
        *big,
    )


def solution(mesh):
    in_specs = (
        P("ep", "tp"),
        P("ep", "tp"),
        P("ep", "tp"),
        P("tp", "ep"),
        P("tp", "ep"),
        P("ep", "tp"),
        P("tp"),
        P(None, "tp"),
        P("ep", "tp"),
        P("ep", None),
        P("ep", None),
        P("ep", "tp", None),
        P("ep", "tp", None),
        P("ep", None, "tp"),
    )
    out_specs = (P("ep", "tp"), P("ep", "tp"))
    return jax.shard_map(body, mesh=mesh, in_specs=in_specs, out_specs=out_specs, check_vma=False)
```

time: 288 us -> 134 us (0.47)
  the two profiles are of different devices: /device:TPU:487 before, /device:TPU:96 now
where the time goes in v1:
time: 134 us
  Pallas kernels  126 us (94%)
  local copies, waits for them, and re-layouts  3.24 us (2%)
  matrix products  2.18 us (2%)
  other arithmetic  1.34 us (1%)
    pallas_call x1, Pallas kernels, body(): pl.pallas_call(functools.partial(kernel, ep, tp, mix_weight.shape[0]), ou...  126 us
    unnamed x2, local copies, waits for them, and re-layouts  3.24 us

profile of v1, /device:TPU:96, one launch (start us, length us, event | category | flops | bytes accessed | tf_op | source)
XLA Modules:
  0.0 133.9 jit_solution(2921250224572041763)
XLA Ops:
  0.7 0.7 broadcast_xor_fusion
  1.3 1.9 %fusion.20 = (f32[1,512]{1,0:T(1,128)}, f32[1,512]{1,0:T(1,128)}) fusion(f32[1,512]{1,0:T(1,128)} %param.17, f32[1,512]{1,0:T(1,128)} %param.18), kind=kOutput, calls=%fused_computation.27 | convolution fusion | flops 3674624 | bytes 8192 | tf_op jit(solution)/shard_map/hs,ts->ht/dot_general | solution.py:698
  3.3 0.2 fusion
  3.5 0.6 select_reduce_fusion
  4.2 126.5 %shard_map.149 = (bf16[512,256]{1,0:T(8,128)(2,1)}, bf16[256,256]{1,0:T(8,128)(2,1)}) custom-call(bf16[256,256]{1,0:T(8,128)(2,1)} %x_ref.1, s32[2,256]{1,0:T(2,128)} %bitcast.17, f32[2,256]{1,0:T(2,128)} %bitcast.18, f32[1,512]{1,0:T(1,128)} %get-tuple-element.2.a_ref, f32[1,512]{1,0:T(1,128)} %get-tuple-element.3.cum_ref, f32[1,256]{1,0:T(1,128)} %bitcast.19, ...), custom_call_target="tpu_custom_call" | custom-call | tf_op jit(solution)/shard_map/pallas_call | solution.py:725
  130.7 1.7 %copy.20 = bf16[512,256]{1,0:T(8,128)(2,1)} copy(bf16[512,256]{1,0:T(8,128)(2,1)} %get-tuple-element.6) | data formatting | bytes 524288
  132.3 1.6 %copy.21 = bf16[256,256]{1,0:T(8,128)(2,1)} copy(bf16[256,256]{1,0:T(8,128)(2,1)} %get-tuple-element.7) | data formatting | bytes 262144
  (3 shorter events, 0.0 us)

commit v2 on v1

v2 whole, which is shorter than its diff:
```python
import functools

import jax
import jax.numpy as jnp
from jax import lax
from jax.experimental import pallas as pl
from jax.experimental.pallas import tpu as pltpu
from jax.sharding import PartitionSpec as P

EPSILON = 1e-06
LOG_FLOOR = -1e30
F32 = jnp.float32
BF16 = jnp.bfloat16
GROUPS = 4
SIDE = 4
PARTS = 2
BLOCK = 4
HEAD = 8
LABEL = 16
FINISH = 5


def flip(index, bits):
    place = 1
    while place <= bits:
        if bits & place:
            index = index + place * (1 - 2 * ((index // place) % 2))
        place *= 2
    return index


def dot(left, right, contract=((1,), (0,))):
    return lax.dot_general(left, right, (contract, ((), ())), preferred_element_type=F32)


def own_mask(size):
    return lax.broadcasted_iota(jnp.int32, (size, size), 0) == lax.broadcasted_iota(
        jnp.int32, (size, size), 1
    )


def upright(row):
    size = row.shape[1]
    return jnp.sum(jnp.where(own_mask(size), row, 0.0), axis=1, keepdims=True)


def flat(column):
    size = column.shape[0]
    return jnp.sum(jnp.where(own_mask(size), column, 0.0), axis=0, keepdims=True)


def kernel(
    ep,
    tp,
    model_width,
    x_hbm,
    routes_hbm,
    weight_hbm,
    in_hbm,
    forget_hbm,
    gain_hbm,
    q_hbm,
    k_hbm,
    v_hbm,
    og_hbm,
    wg_hbm,
    wu_hbm,
    wd_hbm,
    wm_hbm,
    mix_ref,
    exp_ref,
    x_ref,
    routes_ref,
    weight_ref,
    in_ref,
    forget_ref,
    gain_ref,
    q_ref,
    k_ref,
    v_ref,
    og_ref,
    wd_ref,
    wm_ref,
    slot_row_ref,
    a_ref,
    cum_ref,
    wm_turned,
    w1,
    w2,
    slots,
    tok,
    part_own,
    part_out,
    part_in,
    sq_out,
    sq_in,
    hid,
    outb,
    ret,
    hm,
    num_ref,
    den_ref,
    top_ref,
    loc,
    pair_in,
    both,
    earlier,
    other,
    prior,
    down_in,
    near_out,
    near_in,
    carry_out,
    carry_in,
    load_sem,
    own_sem,
    deal_send,
    deal_recv,
    disp_send,
    disp_recv,
    tok_send,
    tok_recv,
    part_send,
    part_recv,
    sq_send,
    sq_recv,
    hid_send,
    hid_recv,
    ret_send,
    ret_recv,
    head_send,
    head_recv,
    pair_send,
    pair_recv,
    down_send,
    down_recv,
    near_send,
    near_recv,
    carry_send,
    carry_recv,
):
    me = lax.axis_index("ep")
    mine = lax.axis_index("tp")
    row, column = mine // SIDE, mine % SIDE
    chip, core = me // 2, me % 2
    chips = ep // 2
    block, place_in_block = chip // BLOCK, chip % BLOCK
    last_block = chips // BLOCK - 1
    cap = slots.shape[0] // ep
    span = slots.shape[0] // GROUPS
    half_span = span // 2
    per = ep // GROUPS
    width = x_ref.shape[1]
    tokens = x_ref.shape[0]
    length, qk = q_ref.shape
    vw = v_ref.shape[1]
    units = wg_hbm.shape[0]
    wide = SIDE * width

    names = (
        (routes_hbm, routes_ref),
        (x_hbm, x_ref),
        (forget_hbm, forget_ref),
        (in_hbm, in_ref),
        (k_hbm, k_ref),
        (v_hbm, v_ref),
        (q_hbm, q_ref),
        (wd_hbm, wd_ref),
        (wm_hbm, wm_ref),
        (og_hbm, og_ref),
        (gain_hbm, gain_ref),
        (weight_hbm, weight_ref),
    )
    loads = [
        pltpu.make_async_copy(source, target, load_sem.at[at])
        for at, (source, target) in enumerate(names)
    ]
    for load in loads:
        load.start()

    def piece(source, j, k):
        start = pl.multiple_of((flip(row, k) * SIDE + flip(column, j)) * width, width)
        return source.at[:, pl.ds(start, width)]

    def slot_of(j, which, k):
        return w1.at[pl.ds((2 * j + which) * units, units), pl.ds(k * width, width)]

    own_pieces = [
        pltpu.make_async_copy(
            piece(source, 0, k), slot_of(0, which, k), own_sem.at[which * SIDE + k]
        )
        for which, source in enumerate((wg_hbm, wu_hbm))
        for k in range(SIDE)
    ]
    for load in own_pieces:
        load.start()

    def deal(j, which, k):
        return pltpu.make_async_remote_copy(
            piece(wu_hbm if which else wg_hbm, j, k),
            slot_of(j, which, k),
            deal_send.at[0],
            deal_recv.at[0],
            device_id={"tp": flip(mine, j)},
        )

    def deals():
        foreign = w1.at[pl.ds(2 * units, 2 * (SIDE - 1) * units)]
        return pltpu.make_async_remote_copy(
            foreign, foreign, deal_send.at[0], deal_recv.at[0], device_id={"tp": flip(mine, 1)}
        )

    dealt = [(j, which, k) for j in range(1, SIDE) for which in range(2) for k in range(SIDE)]

    barrier = pltpu.get_barrier_semaphore()
    for i in range(1, ep):
        pl.semaphore_signal(barrier, inc=1, device_id={"ep": flip(me, i)})
    for j in range(1, tp):
        pl.semaphore_signal(barrier, inc=1, device_id={"tp": flip(mine, j)})

    loads[0].wait()
    experts = lax.broadcasted_iota(jnp.int32, (ep, tokens), 0)
    named = [experts == (routes_ref[route : route + 1, :] ^ me) for route in range(2)]
    any_named = (named[0] | named[1]).astype(F32).astype(BF16)
    older = lax.broadcasted_iota(jnp.int32, (tokens, tokens), 0) < lax.broadcasted_iota(
        jnp.int32, (tokens, tokens), 1
    )
    before = dot(any_named, older.astype(F32).astype(BF16))
    places = (experts * cap).astype(F32) + before
    for route in range(2):
        slot_row_ref[route : route + 1, :] = jnp.sum(
            jnp.where(named[route], places, 0.0), axis=0, keepdims=True
        ).astype(jnp.int32)
    loads[1].wait()

    def pick(group, carry):
        at = group * span
        rows = at + lax.broadcasted_iota(jnp.int32, (span, tokens), 0)
        hit = (rows == slot_row_ref[0:1, :]) | (rows == slot_row_ref[1:2, :])
        chosen = dot(hit.astype(F32).astype(BF16), x_ref[...]).astype(BF16)
        slots[pl.ds(pl.multiple_of(at, span), span), :] = chosen
        return carry

    lax.fori_loop(0, GROUPS, pick, 0)

    with jax.named_scope("barrier"):
        pl.semaphore_wait(barrier, ep - 1 + tp - 1)

    def dispatch(i):
        return pltpu.make_async_remote_copy(
            slots.at[pl.ds(i * cap, cap)],
            tok.at[pl.ds(i * cap, cap), pl.ds(0, width)],
            disp_send.at[0],
            disp_recv.at[i // per],
            device_id={"ep": flip(me, i)},
        )

    def dispatched(group):
        begin = cap if group == 0 else group * span
        rows = pl.ds(begin, (group + 1) * span - begin)
        return pltpu.make_async_remote_copy(
            slots.at[rows],
            tok.at[rows, pl.ds(0, width)],
            disp_send.at[0],
            disp_recv.at[group],
            device_id={"ep": flip(me, 1)},
        )

    def held(i):
        ahead = (flip(chip, i // 2) - chip + chips) % chips
        return (core == 1) & (place_in_block < BLOCK - 1) & (ahead > 0) & (ahead <= chips // 2)

    for i in range(1, ep):

        @pl.when(jnp.logical_not(held(i)))
        def _():
            dispatch(i).start()

    tok[0:cap, 0:width] = slots[0:cap, :]
    for each in dealt:
        deal(*each).start()


    loads[2].wait()
    loads[3].wait()
    gates_in = forget_ref[...]
    log_keep = jnp.minimum(gates_in, 0.0) - jnp.log1p(jnp.exp(-jnp.abs(gates_in)))
    high = log_keep.astype(BF16).astype(F32)
    mid = (log_keep - high).astype(BF16).astype(F32)
    low = log_keep - high - mid
    which_row = lax.broadcasted_iota(jnp.int32, (8, length), 0)
    thirds = jnp.where(
        which_row == 0, high, jnp.where(which_row == 1, mid, jnp.where(which_row == 2, low, 0.0))
    )
    upto = lax.broadcasted_iota(jnp.int32, (length, length), 0) <= lax.broadcasted_iota(
        jnp.int32, (length, length), 1
    )
    sums = dot(thirds.astype(BF16), upto.astype(F32).astype(BF16))
    cum_ref[...] = sums[0:1, :] + sums[1:2, :] + sums[2:3, :]
    a_ref[...] = in_ref[...] - cum_ref[...]

    loads[4].wait()
    loads[5].wait()
    decay = cum_ref[0:1, length - 1 : length]
    log_in = a_ref[0:1, :]
    local_top = jnp.max(log_in, axis=1, keepdims=True)
    weighted = k_ref[...].astype(F32) * jnp.exp(upright(log_in) - local_top)
    loc[HEAD : HEAD + qk, :] = dot(weighted.astype(BF16), v_ref[...], ((0,), (0,)))
    loc[0:HEAD, 0:qk] = jnp.broadcast_to(jnp.sum(weighted, axis=0, keepdims=True), (HEAD, qk))
    loc[0:HEAD, qk:vw] = jnp.broadcast_to(local_top + decay, (HEAD, vw - qk))
    loc[HEAD + qk :, :] = jnp.broadcast_to(decay, (8, vw))

    pair = pltpu.make_async_remote_copy(
        loc, pair_in, pair_send.at[0], pair_recv.at[0], device_id={"ep": flip(me, 1)}
    )

    @pl.when(core == 0)
    def _():
        pair.start()

    def gates(first_max, second_max):
        top = jnp.maximum(first_max, second_max)
        return top, jnp.exp(first_max - top), jnp.exp(second_max - top)

    def merge(target, first, second):
        second_decay = second[HEAD + qk : HEAD + qk + 1, 0:1]
        top, keep, add = gates(
            first[0:1, qk : qk + 1] + second_decay, second[0:1, qk : qk + 1]
        )
        target[0:HEAD, 0:qk] = keep * first[0:HEAD, 0:qk] + add * second[0:HEAD, 0:qk]
        target[0:HEAD, qk:vw] = jnp.broadcast_to(top, (HEAD, vw - qk))
        target[HEAD : HEAD + qk, :] = (
            keep * first[HEAD : HEAD + qk, :] + add * second[HEAD : HEAD + qk, :]
        )
        target[HEAD + qk :, :] = first[HEAD + qk :, :] + second[HEAD + qk :, :]


    def encode(target, source):
        line = lax.broadcasted_iota(jnp.int32, (LABEL, vw), 0)
        label = jnp.zeros((LABEL, vw), F32)
        for base, rest in ((0, source[0:1, :]), (3, source[HEAD + qk : HEAD + qk + 1, :])):
            for at in range(3):
                part = rest.astype(BF16).astype(F32)
                label = jnp.where(line == base + at, part, label)
                rest = rest - part
        target[0:LABEL, :] = label.astype(BF16)
        target[LABEL:, :] = source[HEAD : HEAD + qk, :].astype(BF16)

    def decode(target, source):
        label = source[0:LABEL, :].astype(F32)
        target[0:HEAD, :] = jnp.broadcast_to(label[0:1, :] + label[1:2, :] + label[2:3, :], (HEAD, vw))
        target[HEAD + qk :, :] = jnp.broadcast_to(
            label[3:4, :] + label[4:5, :] + label[5:6, :], (8, vw)
        )
        target[HEAD : HEAD + qk, :] = source[LABEL:, :].astype(F32)

    def near(ahead):
        return pltpu.make_async_remote_copy(
            near_out,
            near_in.at[ahead - 1],
            near_send.at[ahead - 1],
            near_recv.at[ahead - 1],
            device_id={"ep": me + 2 * ahead},
        )

    def carry(ahead):
        return pltpu.make_async_remote_copy(
            carry_out,
            carry_in,
            carry_send.at[ahead - 1],
            carry_recv.at[0],
            device_id={"ep": me + 2 * ahead},
        )

    down = pltpu.make_async_remote_copy(
        other, down_in, down_send.at[0], down_recv.at[0], device_id={"ep": flip(me, 1)}
    )

    @pl.when(core == 1)
    def _():
        pair.wait_recv()
        merge(both, pair_in, loc)
        encode(near_out, both)
        for ahead in range(BLOCK - 1, 0, -1):

            @pl.when(place_in_block + ahead < BLOCK)
            def _():
                near(ahead).start()

    for i in range(1, ep):

        @pl.when(held(i))
        def _():
            dispatch(i).start()

    def gather_block():
        earlier[0:HEAD, 0:qk] = jnp.zeros((HEAD, qk), F32)
        earlier[0:HEAD, qk:vw] = jnp.full((HEAD, vw - qk), LOG_FLOOR, F32)
        earlier[HEAD:, :] = jnp.zeros((qk + 8, vw), F32)
        for ahead in range(BLOCK - 1, 0, -1):

            @pl.when(place_in_block >= ahead)
            def _():
                near(ahead).wait_recv()
                decode(other, near_in.at[ahead - 1])
                merge(earlier, earlier, other)

    sends_carry = (core == 1) & (place_in_block == BLOCK - 1) & (block < last_block)

    def take_carry():
        carry(1).wait_recv()
        decode(other, carry_in)

    def send_carry(number):
        @pl.when(sends_carry & (block == number))
        def _():
            with jax.named_scope("carry"):
                if number > 0:
                    take_carry()
                    merge(other, other, earlier)
                    merge(prior, other, both)
                else:
                    merge(prior, earlier, both)
                encode(carry_out, prior)
                for ahead in range(BLOCK, 0, -1):
                    carry(ahead).start()

    with jax.named_scope("inblock"):
        loads[6].wait()
    tile = length // 4
    scale = qk**-0.5
    for at in range(4):
        rows = pl.ds(at * tile, tile)
        seen = (at + 1) * tile
        causal = lax.broadcasted_iota(jnp.int32, (tile, seen), 1) <= at * tile + (
            lax.broadcasted_iota(jnp.int32, (tile, seen), 0)
        )
        log_seen = jnp.where(causal, a_ref[0:1, 0:seen], -jnp.inf)
        top = jnp.max(log_seen, axis=1, keepdims=True)
        scores = dot(q_ref[rows, :], k_ref[0:seen, :], ((1,), (1,))) * scale
        scores = scores * jnp.exp(log_seen - top)
        num_ref[rows, :] = dot(scores.astype(BF16), v_ref[0:seen, :])
        den_ref[rows, :] = jnp.broadcast_to(jnp.sum(scores, axis=1, keepdims=True), (tile, 128))
        top_ref[rows, :] = jnp.broadcast_to(top, (tile, 128))

    loads[7].wait()
    nothing = jnp.zeros((units, width), BF16)
    for turned in range(2):
        for at in range(tp):
            unit = (at % SIDE) * SIDE + at // SIDE if turned else at
            kept = wd_ref[unit * units : (unit + 1) * units, :]
            first = at * 2 * units
            w2[turned, first : first + units, 0:width] = kept
            w2[turned, first : first + units, width : 2 * width] = nothing
            w2[turned, first + units : first + 2 * units, 0:width] = nothing
            w2[turned, first + units : first + 2 * units, width : 2 * width] = kept
    loads[8].wait()

    def turn_block(at, carry):
        source = pl.multiple_of(((at % SIDE) * SIDE + at // SIDE) * width, width)
        target = pl.multiple_of(at * width, width)
        wm_turned[pl.ds(target, width), :] = wm_ref[pl.ds(source, width), :]
        return carry

    lax.fori_loop(0, tp, turn_block, 0)

    @pl.when(core == 1)
    def _():
        with jax.named_scope("near"):
            gather_block()

    send_carry(0)


    def spread(group, k):
        rows = pl.ds(group * span, span)
        return pltpu.make_async_remote_copy(
            tok.at[rows, pl.ds(0, width)],
            tok.at[rows, pl.ds(k * width, width)],
            tok_send.at[0],
            tok_recv.at[group, k],
            device_id={"tp": flip(mine, SIDE * k)},
        )

    def onward(group, k):
        rows = pl.ds(group * span + (k // 2) * half_span, half_span)
        return pltpu.make_async_remote_copy(
            tok.at[rows, pl.ds(k * width, width)],
            tok.at[rows, pl.ds(2 * width, width)],
            tok_send.at[0],
            tok_recv.at[group, 4 + k],
            device_id={"tp": flip(mine, SIDE * (SIDE - k))},
        )

    def send_partial(group, j):
        rows = pl.ds(group * span, span)
        return pltpu.make_async_remote_copy(
            part_out.at[j, rows],
            part_in.at[j, rows],
            part_send.at[0],
            part_recv.at[group],
            device_id={"tp": flip(mine, j)},
        )

    def send_squares(group, j):
        return pltpu.make_async_remote_copy(
            sq_out.at[group],
            sq_in.at[group, j],
            sq_send.at[0],
            sq_recv.at[group],
            device_id={"tp": flip(mine, j)},
        )

    def partials(group):
        rows = pl.ds(group * span, span)
        return pltpu.make_async_remote_copy(
            part_out.at[pl.ds(1, SIDE - 1), rows],
            part_in.at[pl.ds(1, SIDE - 1), rows],
            part_send.at[0],
            part_recv.at[group],
            device_id={"tp": flip(mine, 1)},
        )

    def squares_of(group):
        foreign = sq_in.at[group, pl.ds(1, SIDE - 1)]
        return pltpu.make_async_remote_copy(
            foreign, foreign, sq_send.at[0], sq_recv.at[group], device_id={"tp": flip(mine, 1)}
        )


    def gather_copies(buffer, first_row, rows, wide_block, x_first, send, recv):
        inner, outer = (column, row) if x_first else (row, column)
        inner_bits, outer_bits = (1, SIDE) if x_first else (SIDE, 1)
        base = outer * SIDE * wide_block
        half = rows // 2

        def cut(part, block, count):
            begin, extent = (first_row, rows) if part is None else (first_row + part * half, half)
            return buffer.at[
                pl.ds(begin, extent),
                pl.ds(pl.multiple_of(base + block * wide_block, wide_block), count * wide_block),
            ]

        def outer_cut(part, bits):
            begin, extent = (first_row, rows) if part is None else (first_row + part * half, half)
            start = pl.multiple_of(flip(outer, bits) * SIDE * wide_block, SIDE * wide_block)
            return buffer.at[pl.ds(begin, extent), pl.ds(start, SIDE * wide_block)]

        def remote(piece_of, at, bits):
            return pltpu.make_async_remote_copy(
                piece_of, piece_of, send, recv.at[at], device_id={"tp": flip(mine, bits)}
            )

        def inner_send(k):
            return remote(cut(None, inner, 1), k // 2, k * inner_bits)

        def inner_relay(k):
            return remote(
                cut(k // 2, flip(inner, k), 1), 2 + k // 2, (SIDE - k) * inner_bits
            )

        def outer_send(k):
            return remote(outer_cut(None, 0), 4 + k // 2, k * outer_bits)

        def outer_relay(k):
            return remote(outer_cut(k // 2, k), 6 + k // 2, (SIDE - k) * outer_bits)

        return [[make(k) for k in (1, 3)] for make in (inner_send, inner_relay, outer_send, outer_relay)]

    def gather_step(copies, step):
        if step > 0:
            for copy in copies[step - 1]:
                copy.wait_recv()
        if step < 4:
            for copy in copies[step]:
                copy.start()

    hid_copies = [
        gather_copies(
            hid,
            group * half_span,
            half_span,
            2 * units,
            group % 2 == 0,
            hid_send.at[0],
            hid_recv.at[group],
        )
        for group in range(GROUPS)
    ]

    def give_back(i):
        return pltpu.make_async_remote_copy(
            outb.at[pl.ds(i * cap, cap)],
            ret.at[pl.ds(i * cap, cap)],
            ret_send.at[0],
            ret_recv.at[i // per],
            device_id={"ep": flip(me, i)},
        )

    def given_back(group):
        begin = cap if group == 0 else group * span
        rows = pl.ds(begin, (group + 1) * span - begin)
        return pltpu.make_async_remote_copy(
            outb.at[rows], ret.at[rows], ret_send.at[0], ret_recv.at[group], device_id={"ep": flip(me, 1)}
        )

    def stage(group, step):
        rows = pl.ds(group * span, span)
        packed = pl.ds(group * half_span, half_span)
        if step == 0:
            dispatched(group).wait_recv()
            for k in (1, 3):
                spread(group, k).start()
        elif step == 1:
            for k in (1, 3):
                spread(group, k).wait_recv()
                onward(group, k).start()
        elif step == 2:
            if group == 0:
                for load in own_pieces:
                    load.wait()
                deals().wait_recv()
            for k in (1, 3):
                onward(group, k).wait_recv()
            piece_of = tok[rows, :]
            partial = dot(piece_of, w1[...], ((1,), (1,)))
            part_own[rows, :] = partial[:, 0 : 2 * units]
            for j in range(1, SIDE):
                part_out[j, rows, :] = partial[:, j * 2 * units : (j + 1) * 2 * units].astype(BF16)
            for j in range(1, SIDE):
                send_partial(group, j).start()
            full = piece_of.astype(F32)
            squares = flat(jnp.sum(full * full, axis=1, keepdims=True))
            sq_out[group] = jnp.broadcast_to(squares, (8, span))
            for j in range(1, SIDE):
                send_squares(group, j).start()
        elif step == 3:
            squares = sq_out[group][0:1, :]
            squares_of(group).wait_recv()
            for j in range(1, SIDE):
                squares = squares + sq_in[group, j][0:1, :]
            inverse = upright(lax.rsqrt(squares / model_width + EPSILON))
            total = part_own[rows, :]
            partials(group).wait_recv()
            for j in range(1, SIDE):
                total = total + part_in[j, rows, :].astype(F32)
            total = total * inverse
            hidden = jax.nn.silu(total) * pltpu.roll(total, units, 1)
            turned = pltpu.roll(hidden, units, 1)
            lanes = lax.broadcasted_iota(jnp.int32, (half_span, 2 * units), 1)
            both_rows = jnp.where(lanes < units, hidden[0:half_span, :], turned[half_span:span, :])
            place = mine if group % 2 == 0 else column * SIDE + row
            columns = pl.ds(pl.multiple_of(place * 2 * units, 2 * units), 2 * units)
            hid[packed, columns] = both_rows.astype(BF16)
            gather_step(hid_copies[group], 0)
        elif step < 7:
            gather_step(hid_copies[group], step - 3)
        else:
            gather_step(hid_copies[group], 4)
            total = dot(hid[packed, :], w2[group % 2])
            outb[pl.ds(group * span, half_span), :] = total[:, 0:width].astype(BF16)
            outb[pl.ds(group * span + half_span, half_span), :] = total[:, width:].astype(BF16)
            for i in range(max(1, group * per), (group + 1) * per):
                give_back(i).start()

    part_rows = length // (2 * PARTS)
    head_copies = [
        gather_copies(
            hm.at[at // PARTS],
            (at % PARTS) * part_rows,
            part_rows,
            width,
            at // PARTS == 0,
            head_send.at[0],
            head_recv.at[at],
        )
        for at in range(2 * PARTS)
    ]
    orders = [at // 2 + (at % 2) * PARTS for at in range(2 * PARTS)]


    def take_prior():
        @pl.when(core == 1)
        def _():
            @pl.when((block > 0) & jnp.logical_not(sends_carry))
            def _():
                take_carry()
                merge(other, other, earlier)

            @pl.when(block == 0)
            def _():
                other[...] = earlier[...]

            down.start()
            merge(prior, other, pair_in)

        @pl.when(core == 0)
        def _():
            down.wait_recv()
            prior[...] = down_in[...]

        for load in loads[9:11]:
            load.wait()

    def finish_heads():
        prior_max = prior[0:1, qk : qk + 1]
        normal = prior[0:1, 0:qk]
        memory = prior[HEAD : HEAD + qk, :]
        high = memory.astype(BF16)
        low = (memory - high.astype(F32)).astype(BF16)
        for at in orders:
            rows = pl.ds(at * part_rows, part_rows)
            queries = q_ref[rows, :]
            own_top = top_ref[rows, 0:1]
            top = jnp.maximum(prior_max, own_top)
            again = jnp.exp(own_top - top)
            carried = jnp.exp(prior_max - top) * scale
            numerator = carried * (dot(queries, high) + dot(queries, low)) + again * num_ref[rows, :]
            denominator = (
                carried * jnp.sum(queries.astype(F32) * normal, axis=1, keepdims=True)
                + again * den_ref[rows, 0:1]
            )
            cumulative = upright(cum_ref[0:1, at * part_rows : (at + 1) * part_rows])
            floor = jnp.exp(-(cumulative + top))
            value = numerator / jnp.maximum(jnp.abs(denominator), floor)
            value = value * lax.rsqrt(jnp.mean(value * value, axis=1, keepdims=True) + EPSILON)
            gate = jax.nn.sigmoid(og_ref[rows, :].astype(F32))
            place = mine if at < PARTS else column * SIDE + row
            hm[
                at // PARTS,
                pl.ds((at % PARTS) * part_rows, part_rows),
                pl.ds(pl.multiple_of(place * width, width), width),
            ] = (value * gain_ref[...] * gate).astype(BF16)
            gather_step(head_copies[at], 0)

    def head_step(step):
        for at in orders:
            gather_step(head_copies[at], step)
            if step == 4:
                inputs = hm[at // PARTS, pl.ds((at % PARTS) * part_rows, part_rows), :]
                weights = wm_ref if at < PARTS else wm_turned
                mix_ref[pl.ds(at * part_rows, part_rows), :] = dot(inputs, weights[...]).astype(BF16)

    ticks = GROUPS + 7
    for tick in range(ticks):
        if tick == FINISH:
            with jax.named_scope("prior"):
                take_prior()
            with jax.named_scope("heads"):
                finish_heads()
        for group in range(GROUPS):
            if 0 <= tick - group < 8:
                with jax.named_scope(f"stage{group}_{tick - group}"):
                    stage(group, tick - group)
            if tick == 1 and group < 2:
                send_carry(group + 1)
        if FINISH < tick < FINISH + 5:
            with jax.named_scope(f"gather{tick - FINISH}"):
                head_step(tick - FINISH)
    ret[0:cap, :] = outb[0:cap, :]

    total = jnp.zeros((tokens, width), F32)
    places = lax.broadcasted_iota(jnp.int32, (span, tokens), 0)
    loads[11].wait()
    weights = [upright(weight_ref[route : route + 1, :]) for route in range(weight_ref.shape[0])]
    for group in range(GROUPS):
        with jax.named_scope(f"back{group}"):
            given_back(group).wait_recv()
        rows = pl.ds(group * span, span)
        for route, weight in enumerate(weights):
            hit = places == slot_row_ref[route : route + 1, :] - group * span
            picked = dot(hit.astype(F32).astype(BF16), ret[rows, :], ((0,), (0,)))
            total += picked * weight
    exp_ref[...] = total.astype(BF16)

    def sent(source, semaphore):
        pltpu.make_async_remote_copy(
            source, source, semaphore, semaphore, device_id={"ep": flip(me, 1)}
        ).wait_send()

    with jax.named_scope("drain"):
        foreign = pl.ds(cap, slots.shape[0] - cap)
        sent(slots.at[foreign], disp_send.at[0])
        sent(outb.at[foreign], ret_send.at[0])
        deals().wait_send()
        sent(tok.at[:, pl.ds(0, 3 * width)], tok_send.at[0])
        sent(part_out.at[pl.ds(1, SIDE - 1)], part_send.at[0])
        sent(sq_in.at[:, pl.ds(1, SIDE - 1)], sq_send.at[0])
        sent(hid.at[:, pl.ds(0, (tp - 1) * 2 * units)], hid_send.at[0])
        for part in range(2):
            sent(hm.at[part, :, pl.ds(0, (tp - 1) * width)], head_send.at[0])

    @pl.when(core == 0)
    def _():
        pair.wait_send()

    @pl.when(core == 1)
    def _():
        down.wait_send()
        for ahead in range(1, BLOCK):

            @pl.when(place_in_block + ahead < BLOCK)
            def _():
                near(ahead).wait_send()

    @pl.when(sends_carry)
    def _():
        for ahead in range(1, BLOCK + 1):
            carry(ahead).wait_send()


def body(
    query_rows,
    key_rows,
    value_rows,
    in_gate,
    forget_gate,
    out_gate,
    head_gain,
    mix_weight,
    expert_input,
    routes,
    route_weight,
    gate_weight,
    up_weight,
    down_weight,
):
    ep, tp = lax.axis_size("ep"), lax.axis_size("tp")
    length = in_gate.shape[1]
    token_count, fanout = routes.shape
    width = expert_input.shape[1]
    units = gate_weight.shape[1]
    capacity = 2 * token_count * fanout // ep
    slot_count = ep * capacity
    qk = query_rows.shape[1]
    vw = value_rows.shape[1]

    vmem = pl.BlockSpec(memory_space=pltpu.VMEM)
    anywhere = pl.BlockSpec(memory_space=pl.ANY)
    dma = pltpu.SemaphoreType.DMA
    gate_local, up_local, down_local = gate_weight[0], up_weight[0], down_weight[0]
    small = (expert_input, routes.T, route_weight.T, in_gate, forget_gate, head_gain[None, :])
    big = (query_rows, key_rows, value_rows, out_gate, gate_local, up_local, down_local, mix_weight)
    held = (query_rows, key_rows, value_rows, out_gate, down_local, mix_weight)
    tall = (HEAD + qk + 8, vw)
    message = (LABEL + qk, vw)
    return pl.pallas_call(
        functools.partial(kernel, ep, tp, mix_weight.shape[0]),
        out_shape=(
            jax.ShapeDtypeStruct((length, width), BF16),
            jax.ShapeDtypeStruct((token_count, width), BF16),
        ),
        in_specs=[anywhere] * 14,
        out_specs=(vmem, vmem),
        scratch_shapes=[pltpu.VMEM(array.shape, array.dtype) for array in small + held]
        + [
            pltpu.VMEM((fanout, token_count), jnp.int32),
            pltpu.VMEM((1, length), F32),
            pltpu.VMEM((1, length), F32),
            pltpu.VMEM(mix_weight.shape, BF16),
            pltpu.VMEM((SIDE * 2 * units, SIDE * width), BF16),
            pltpu.VMEM((2, tp * 2 * units, 2 * width), BF16),
            pltpu.VMEM((slot_count, width), BF16),
            pltpu.VMEM((slot_count, SIDE * width), BF16),
            pltpu.VMEM((slot_count, 2 * units), F32),
            pltpu.VMEM((SIDE, slot_count, 2 * units), BF16),
            pltpu.VMEM((SIDE, slot_count, 2 * units), BF16),
            pltpu.VMEM((GROUPS, 8, slot_count // GROUPS), F32),
            pltpu.VMEM((GROUPS, SIDE, 8, slot_count // GROUPS), F32),
            pltpu.VMEM((slot_count // 2, tp * 2 * units), BF16),
            pltpu.VMEM((slot_count, width), BF16),
            pltpu.VMEM((slot_count, width), BF16),
            pltpu.VMEM((2, length // 2, tp * width), BF16),
            pltpu.VMEM((length, vw), F32),
            pltpu.VMEM((length, 128), F32),
            pltpu.VMEM((length, 128), F32),
            pltpu.VMEM(tall, F32),
            pltpu.VMEM(tall, F32),
            pltpu.VMEM(tall, F32),
            pltpu.VMEM(tall, F32),
            pltpu.VMEM(tall, F32),
            pltpu.VMEM(tall, F32),
            pltpu.VMEM(tall, F32),
            pltpu.VMEM(message, BF16),
            pltpu.VMEM((BLOCK - 1, *message), BF16),
            pltpu.VMEM(message, BF16),
            pltpu.VMEM(message, BF16),
            dma((12,)),
            dma((2 * SIDE,)),
            dma((1,)),
            dma((1,)),
            dma((1,)),
            dma((GROUPS,)),
            dma((1,)),
            dma((GROUPS, 8)),
            dma((1,)),
            dma((GROUPS,)),
            dma((1,)),
            dma((GROUPS,)),
            dma((1,)),
            dma((GROUPS, 8)),
            dma((1,)),
            dma((GROUPS,)),
            dma((1,)),
            dma((2 * PARTS, 8)),
            dma((1,)),
            dma((1,)),
            dma((1,)),
            dma((1,)),
            dma((BLOCK - 1,)),
            dma((BLOCK - 1,)),
            dma((BLOCK,)),
            dma((1,)),
        ],
        compiler_params=pltpu.CompilerParams(
            collective_id=0, has_side_effects=True, vmem_limit_bytes=64000 * 1024
        ),
    )(*small, *big)


def solution(mesh):
    in_specs = (
        P("ep", "tp"),
        P("ep", "tp"),
        P("ep", "tp"),
        P("tp", "ep"),
        P("tp", "ep"),
        P("ep", "tp"),
        P("tp"),
        P(None, "tp"),
        P("ep", "tp"),
        P("ep", None),
        P("ep", None),
        P("ep", "tp", None),
        P("ep", "tp", None),
        P("ep", None, "tp"),
    )
    out_specs = (P("ep", "tp"), P("ep", "tp"))
    return jax.shard_map(body, mesh=mesh, in_specs=in_specs, out_specs=out_specs, check_vma=False)
```

time: 134 us -> 121 us (0.903)
  the two profiles are of different devices: /device:TPU:96 before, /device:TPU:1 now
where the time goes in v2:
time: 121 us
  Pallas kernels  117 us (97%)
  local copies, waits for them, and re-layouts  3.24 us (3%)
    pallas_call x1, Pallas kernels, body(): pl.pallas_call(functools.partial(kernel, ep, tp, mix_weight.shape[0]), ou...  117 us
    unnamed x2, local copies, waits for them, and re-layouts  3.24 us

profile of v2, /device:TPU:1, one launch (start us, length us, event | category | flops | bytes accessed | tf_op | source)
XLA Modules:
  0.0 120.8 jit_solution(9119413711150773663)
XLA Ops:
  0.6 116.9 %shard_map.149 = (bf16[512,256]{1,0:T(8,128)(2,1)}, bf16[256,256]{1,0:T(8,128)(2,1)}) custom-call(bf16[256,256]{1,0:T(8,128)(2,1)} %x_hbm.1, s32[2,256]{1,0:T(2,128)} %bitcast.9, f32[2,256]{1,0:T(2,128)} %bitcast.10, f32[1,512]{1,0:T(1,128)} %in_hbm.1, f32[1,512]{1,0:T(1,128)} %forget_hbm.1, f32[1,256]{1,0:T(1,128)} %bitcast.11, bf16[512,128]{1,0:T(8,128)(2,1)} %q_hbm.1, ...), custom_call_target="tpu_custom_call" | custom-call | tf_op jit(solution)/shard_map/pallas_call | solution.py:847
  117.5 1.7 %copy.18 = bf16[512,256]{1,0:T(8,128)(2,1)} copy(bf16[512,256]{1,0:T(8,128)(2,1)} %get-tuple-element.4) | data formatting | bytes 524288
  119.2 1.6 %copy.19 = bf16[256,256]{1,0:T(8,128)(2,1)} copy(bf16[256,256]{1,0:T(8,128)(2,1)} %get-tuple-element.5) | data formatting | bytes 262144

commit v3 on v2

--- a/solution.py
+++ b/solution.py
@@ -13,11 +13,17 @@
 BF16 = jnp.bfloat16
 GROUPS = 4
 SIDE = 4
-PARTS = 2
+PARTS = 4
 BLOCK = 4
 HEAD = 8
 LABEL = 16
-FINISH = 5
+SEQUENCE = (
+    "s00", "d0", "s01", "s10", "h0", "s02", "s20", "s11", "near", "s03", "s21", "s30", "s12",
+    "carry1", "s04", "s22", "s31", "build", "s13", "s05", "carry2", "s23", "s14", "s32", "s24",
+    "s06", "d1", "heads", "s15", "g0", "s33", "s25", "s16", "g1", "s34", "g2", "h1", "g3", "m0",
+    "s26", "s35", "m1", "m2", "m3", "s36", "f0", "f1", "f2", "f3",
+)
+ORDER = (0, 3, -3, 4, 8, 7, -7, -6, 6, 5, -5, -4, 2, 1, -1, -2)
 
 
 def flip(index, bits):
@@ -80,12 +86,11 @@
     v_ref,
     og_ref,
     wd_ref,
-    wm_ref,
     slot_row_ref,
     a_ref,
     cum_ref,
-    wm_turned,
     w1,
+    wmix,
     w2,
     slots,
     tok,
@@ -98,6 +103,9 @@
     outb,
     ret,
     hm,
+    mix_own,
+    mix_out,
+    mix_in,
     num_ref,
     den_ref,
     top_ref,
@@ -116,6 +124,10 @@
     own_sem,
     deal_send,
     deal_recv,
+    mix_deal_send,
+    mix_deal_recv,
+    hand_send,
+    hand_recv,
     disp_send,
     disp_recv,
     tok_send,
@@ -130,6 +142,8 @@
     ret_recv,
     head_send,
     head_recv,
+    mix_send,
+    mix_recv,
     pair_send,
     pair_recv,
     down_send,
@@ -166,7 +180,6 @@
         (v_hbm, v_ref),
         (q_hbm, q_ref),
         (wd_hbm, wd_ref),
-        (wm_hbm, wm_ref),
         (og_hbm, og_ref),
         (gain_hbm, gain_ref),
         (weight_hbm, weight_ref),
@@ -192,8 +205,48 @@
         for which, source in enumerate((wg_hbm, wu_hbm))
         for k in range(SIDE)
     ]
+
+    def mix_piece(j, k):
+        turned = row + (k % 2) * (1 - 2 * (row % 2)) + 2 * (k // 2) * (1 - 2 * (row // 2 % 2))
+        start = pl.multiple_of((turned * SIDE + flip(column, j)) * width, width)
+        return wm_hbm.at[pl.ds(start, width), :]
+
+    def mix_slot(j, k):
+        return wmix.at[pl.ds(pl.multiple_of(k * width, width), width), pl.ds(j * width, width)]
+
+    own_pieces += [
+        pltpu.make_async_copy(mix_piece(0, k), mix_slot(0, k), own_sem.at[2 * SIDE + k])
+        for k in range(SIDE)
+    ]
     for load in own_pieces:
         load.start()
+
+
+    def deal_mix(j, at):
+        k = core + 2 * at
+        return pltpu.make_async_remote_copy(
+            mix_piece(j, k),
+            mix_slot(j, k),
+            mix_deal_send.at[0],
+            mix_deal_recv.at[at],
+            device_id={"tp": flip(mine, j)},
+        )
+
+    def foreign_rows(k):
+        start = pl.multiple_of(k * width, width)
+        return wmix.at[pl.ds(start, width), pl.ds(width, (SIDE - 1) * width)]
+
+    def mix_dealt(at):
+        foreign = foreign_rows(core + 2 * at)
+        return pltpu.make_async_remote_copy(
+            foreign, foreign, mix_deal_send.at[0], mix_deal_recv.at[at], device_id={"tp": flip(mine, 1)}
+        )
+
+    def hand_mix(at, whose):
+        foreign = foreign_rows(whose + 2 * at)
+        return pltpu.make_async_remote_copy(
+            foreign, foreign, hand_send.at[at], hand_recv.at[at], device_id={"ep": flip(me, 1)}
+        )
 
     def deal(j, which, k):
         return pltpu.make_async_remote_copy(
@@ -220,7 +273,17 @@
 
     loads[0].wait()
     experts = lax.broadcasted_iota(jnp.int32, (ep, tokens), 0)
-    named = [experts == (routes_ref[route : route + 1, :] ^ me) for route in range(2)]
+
+    offsets = ORDER if chips == len(ORDER) else tuple(range(chips))
+
+    def turn_of(expert):
+        ahead = ((expert >> 1) - chip) & (chips - 1)
+        step = jnp.zeros_like(ahead)
+        for at, ahead_of in enumerate(offsets):
+            step = jnp.where(ahead == ahead_of % chips, at, step)
+        return 2 * step + ((expert & 1) ^ core)
+
+    named = [experts == turn_of(routes_ref[route : route + 1, :]) for route in range(2)]
     any_named = (named[0] | named[1]).astype(F32).astype(BF16)
     older = lax.broadcasted_iota(jnp.int32, (tokens, tokens), 0) < lax.broadcasted_iota(
         jnp.int32, (tokens, tokens), 1
@@ -246,13 +309,16 @@
     with jax.named_scope("barrier"):
         pl.semaphore_wait(barrier, ep - 1 + tp - 1)
 
+    def peer(i, sign):
+        return 2 * ((chip + sign * offsets[i // 2] + chips) % chips) + (core + i) % 2
+
     def dispatch(i):
         return pltpu.make_async_remote_copy(
             slots.at[pl.ds(i * cap, cap)],
             tok.at[pl.ds(i * cap, cap), pl.ds(0, width)],
             disp_send.at[0],
             disp_recv.at[i // per],
-            device_id={"ep": flip(me, i)},
+            device_id={"ep": peer(i, 1)},
         )
 
     def dispatched(group):
@@ -266,15 +332,8 @@
             device_id={"ep": flip(me, 1)},
         )
 
-    def held(i):
-        ahead = (flip(chip, i // 2) - chip + chips) % chips
-        return (core == 1) & (place_in_block < BLOCK - 1) & (ahead > 0) & (ahead <= chips // 2)
-
     for i in range(1, ep):
-
-        @pl.when(jnp.logical_not(held(i)))
-        def _():
-            dispatch(i).start()
+        dispatch(i).start()
 
     tok[0:cap, 0:width] = slots[0:cap, :]
     for each in dealt:
@@ -387,12 +446,6 @@
             def _():
                 near(ahead).start()
 
-    for i in range(1, ep):
-
-        @pl.when(held(i))
-        def _():
-            dispatch(i).start()
-
     def gather_block():
         earlier[0:HEAD, 0:qk] = jnp.zeros((HEAD, qk), F32)
         earlier[0:HEAD, qk:vw] = jnp.full((HEAD, vw - qk), LOG_FLOOR, F32)
@@ -443,33 +496,17 @@
         den_ref[rows, :] = jnp.broadcast_to(jnp.sum(scores, axis=1, keepdims=True), (tile, 128))
         top_ref[rows, :] = jnp.broadcast_to(top, (tile, 128))
 
-    loads[7].wait()
-    nothing = jnp.zeros((units, width), BF16)
-    for turned in range(2):
+
+    def build_down():
+        loads[7].wait()
+        nothing = jnp.zeros((units, width), BF16)
         for at in range(tp):
-            unit = (at % SIDE) * SIDE + at // SIDE if turned else at
-            kept = wd_ref[unit * units : (unit + 1) * units, :]
+            kept = wd_ref[at * units : (at + 1) * units, :]
             first = at * 2 * units
-            w2[turned, first : first + units, 0:width] = kept
-            w2[turned, first : first + units, width : 2 * width] = nothing
-            w2[turned, first + units : first + 2 * units, 0:width] = nothing
-            w2[turned, first + units : first + 2 * units, width : 2 * width] = kept
-    loads[8].wait()
-
-    def turn_block(at, carry):
-        source = pl.multiple_of(((at % SIDE) * SIDE + at // SIDE) * width, width)
-        target = pl.multiple_of(at * width, width)
-        wm_turned[pl.ds(target, width), :] = wm_ref[pl.ds(source, width), :]
-        return carry
-
-    lax.fori_loop(0, tp, turn_block, 0)
-
-    @pl.when(core == 1)
-    def _():
-        with jax.named_scope("near"):
-            gather_block()
-
-    send_carry(0)
+            w2[first : first + units, 0:width] = kept
+            w2[first : first + units, width : 2 * width] = nothing
+            w2[first + units : first + 2 * units, 0:width] = nothing
+            w2[first + units : first + 2 * units, width : 2 * width] = kept
 
 
     def spread(group, k):
@@ -478,7 +515,7 @@
             tok.at[rows, pl.ds(0, width)],
             tok.at[rows, pl.ds(k * width, width)],
             tok_send.at[0],
-            tok_recv.at[group, k],
+            tok_recv.at[group, k // 2],
             device_id={"tp": flip(mine, SIDE * k)},
         )
 
@@ -488,7 +525,7 @@
             tok.at[rows, pl.ds(k * width, width)],
             tok.at[rows, pl.ds(2 * width, width)],
             tok_send.at[0],
-            tok_recv.at[group, 4 + k],
+            tok_recv.at[group, 2 + k // 2],
             device_id={"tp": flip(mine, SIDE * (SIDE - k))},
         )
 
@@ -528,65 +565,47 @@
         )
 
 
-    def gather_copies(buffer, first_row, rows, wide_block, x_first, send, recv):
-        inner, outer = (column, row) if x_first else (row, column)
-        inner_bits, outer_bits = (1, SIDE) if x_first else (SIDE, 1)
-        base = outer * SIDE * wide_block
-        half = rows // 2
-
-        def cut(part, block, count):
-            begin, extent = (first_row, rows) if part is None else (first_row + part * half, half)
-            return buffer.at[
-                pl.ds(begin, extent),
-                pl.ds(pl.multiple_of(base + block * wide_block, wide_block), count * wide_block),
-            ]
-
-        def outer_cut(part, bits):
-            begin, extent = (first_row, rows) if part is None else (first_row + part * half, half)
-            start = pl.multiple_of(flip(outer, bits) * SIDE * wide_block, SIDE * wide_block)
-            return buffer.at[pl.ds(begin, extent), pl.ds(start, SIDE * wide_block)]
-
-        def remote(piece_of, at, bits):
-            return pltpu.make_async_remote_copy(
-                piece_of, piece_of, send, recv.at[at], device_id={"tp": flip(mine, bits)}
-            )
-
-        def inner_send(k):
-            return remote(cut(None, inner, 1), k // 2, k * inner_bits)
-
-        def inner_relay(k):
-            return remote(
-                cut(k // 2, flip(inner, k), 1), 2 + k // 2, (SIDE - k) * inner_bits
-            )
-
-        def outer_send(k):
-            return remote(outer_cut(None, 0), 4 + k // 2, k * outer_bits)
-
-        def outer_relay(k):
-            return remote(outer_cut(k // 2, k), 6 + k // 2, (SIDE - k) * outer_bits)
-
-        return [[make(k) for k in (1, 3)] for make in (inner_send, inner_relay, outer_send, outer_relay)]
-
-    def gather_step(copies, step):
-        if step > 0:
-            for copy in copies[step - 1]:
-                copy.wait_recv()
-        if step < 4:
-            for copy in copies[step]:
-                copy.start()
-
-    hid_copies = [
-        gather_copies(
-            hid,
-            group * half_span,
-            half_span,
-            2 * units,
-            group % 2 == 0,
+    def hid_block(group, at, count):
+        return hid.at[
+            pl.ds(group * half_span, half_span),
+            pl.ds(pl.multiple_of(at * 2 * units, 2 * units), count * 2 * units),
+        ]
+
+    def hid_inner(group, k):
+        block_of = hid_block(group, mine, 1)
+        return pltpu.make_async_remote_copy(
+            block_of, block_of, hid_send.at[0], hid_recv.at[group, 0], device_id={"tp": flip(mine, k)}
+        )
+
+    def hid_outer(group, k):
+        block_of = hid_block(group, row * SIDE, SIDE)
+        return pltpu.make_async_remote_copy(
+            block_of,
+            block_of,
             hid_send.at[0],
-            hid_recv.at[group],
-        )
-        for group in range(GROUPS)
-    ]
+            hid_recv.at[group, 1 + k // 2],
+            device_id={"tp": flip(mine, SIDE * k)},
+        )
+
+    def hid_onward(group, k):
+        quarter = half_span // 2
+        block_of = hid.at[
+            pl.ds(group * half_span + (k // 2) * quarter, quarter),
+            pl.ds(pl.multiple_of(flip(row, k) * SIDE * 2 * units, SIDE * 2 * units), SIDE * 2 * units),
+        ]
+        return pltpu.make_async_remote_copy(
+            block_of,
+            block_of,
+            hid_send.at[0],
+            hid_recv.at[group, 3 + k // 2],
+            device_id={"tp": flip(mine, SIDE * (SIDE - k))},
+        )
+
+    def hid_row(group):
+        foreign = hid_block(group, 0, SIDE - 1)
+        return pltpu.make_async_remote_copy(
+            foreign, foreign, hid_send.at[0], hid_recv.at[group, 0], device_id={"tp": flip(mine, 1)}
+        )
 
     def give_back(i):
         return pltpu.make_async_remote_copy(
@@ -594,7 +613,7 @@
             ret.at[pl.ds(i * cap, cap)],
             ret_send.at[0],
             ret_recv.at[i // per],
-            device_id={"ep": flip(me, i)},
+            device_id={"ep": peer(i, -1)},
         )
 
     def given_back(group):
@@ -617,7 +636,7 @@
                 onward(group, k).start()
         elif step == 2:
             if group == 0:
-                for load in own_pieces:
+                for load in own_pieces[0 : 2 * SIDE]:
                     load.wait()
                 deals().wait_recv()
             for k in (1, 3):
@@ -649,34 +668,60 @@
             turned = pltpu.roll(hidden, units, 1)
             lanes = lax.broadcasted_iota(jnp.int32, (half_span, 2 * units), 1)
             both_rows = jnp.where(lanes < units, hidden[0:half_span, :], turned[half_span:span, :])
-            place = mine if group % 2 == 0 else column * SIDE + row
-            columns = pl.ds(pl.multiple_of(place * 2 * units, 2 * units), 2 * units)
+            columns = pl.ds(pl.multiple_of(mine * 2 * units, 2 * units), 2 * units)
             hid[packed, columns] = both_rows.astype(BF16)
-            gather_step(hid_copies[group], 0)
-        elif step < 7:
-            gather_step(hid_copies[group], step - 3)
+            for k in range(1, SIDE):
+                hid_inner(group, k).start()
+        elif step == 4:
+            hid_row(group).wait_recv()
+            for k in (1, 3):
+                hid_outer(group, k).start()
+        elif step == 5:
+            for k in (1, 3):
+                hid_outer(group, k).wait_recv()
+                hid_onward(group, k).start()
         else:
-            gather_step(hid_copies[group], 4)
-            total = dot(hid[packed, :], w2[group % 2])
+            for k in (1, 3):
+                hid_onward(group, k).wait_recv()
+            total = dot(hid[packed, :], w2[...])
             outb[pl.ds(group * span, half_span), :] = total[:, 0:width].astype(BF16)
             outb[pl.ds(group * span + half_span, half_span), :] = total[:, width:].astype(BF16)
             for i in range(max(1, group * per), (group + 1) * per):
                 give_back(i).start()
 
-    part_rows = length // (2 * PARTS)
-    head_copies = [
-        gather_copies(
-            hm.at[at // PARTS],
-            (at % PARTS) * part_rows,
-            part_rows,
-            width,
-            at // PARTS == 0,
+    part_rows = length // PARTS
+
+    def head_spread(at, k):
+        rows = pl.ds(at * part_rows, part_rows)
+        return pltpu.make_async_remote_copy(
+            hm.at[rows, pl.ds(0, width)],
+            hm.at[rows, pl.ds(k * width, width)],
             head_send.at[0],
             head_recv.at[at],
-        )
-        for at in range(2 * PARTS)
-    ]
-    orders = [at // 2 + (at % 2) * PARTS for at in range(2 * PARTS)]
+            device_id={"tp": flip(mine, SIDE * k)},
+        )
+
+    def heads_of(at):
+        foreign = hm.at[pl.ds(at * part_rows, part_rows), pl.ds(width, (SIDE - 1) * width)]
+        return pltpu.make_async_remote_copy(
+            foreign, foreign, head_send.at[0], head_recv.at[at], device_id={"tp": flip(mine, 1)}
+        )
+
+    def mix_partial(at, j):
+        rows = pl.ds(at * part_rows, part_rows)
+        return pltpu.make_async_remote_copy(
+            mix_out.at[j, rows],
+            mix_in.at[j, rows],
+            mix_send.at[0],
+            mix_recv.at[at],
+            device_id={"tp": flip(mine, j)},
+        )
+
+    def mix_partials(at):
+        foreign = mix_in.at[pl.ds(1, SIDE - 1), pl.ds(at * part_rows, part_rows)]
+        return pltpu.make_async_remote_copy(
+            foreign, foreign, mix_send.at[0], mix_recv.at[at], device_id={"tp": flip(mine, 1)}
+        )
 
 
     def take_prior():
@@ -699,69 +744,103 @@
             down.wait_recv()
             prior[...] = down_in[...]
 
-        for load in loads[9:11]:
+        for load in loads[8:10]:
             load.wait()
 
-    def finish_heads():
+    def finish_heads(at):
         prior_max = prior[0:1, qk : qk + 1]
         normal = prior[0:1, 0:qk]
         memory = prior[HEAD : HEAD + qk, :]
         high = memory.astype(BF16)
         low = (memory - high.astype(F32)).astype(BF16)
-        for at in orders:
-            rows = pl.ds(at * part_rows, part_rows)
-            queries = q_ref[rows, :]
-            own_top = top_ref[rows, 0:1]
-            top = jnp.maximum(prior_max, own_top)
-            again = jnp.exp(own_top - top)
-            carried = jnp.exp(prior_max - top) * scale
-            numerator = carried * (dot(queries, high) + dot(queries, low)) + again * num_ref[rows, :]
-            denominator = (
-                carried * jnp.sum(queries.astype(F32) * normal, axis=1, keepdims=True)
-                + again * den_ref[rows, 0:1]
-            )
-            cumulative = upright(cum_ref[0:1, at * part_rows : (at + 1) * part_rows])
-            floor = jnp.exp(-(cumulative + top))
-            value = numerator / jnp.maximum(jnp.abs(denominator), floor)
-            value = value * lax.rsqrt(jnp.mean(value * value, axis=1, keepdims=True) + EPSILON)
-            gate = jax.nn.sigmoid(og_ref[rows, :].astype(F32))
-            place = mine if at < PARTS else column * SIDE + row
-            hm[
-                at // PARTS,
-                pl.ds((at % PARTS) * part_rows, part_rows),
-                pl.ds(pl.multiple_of(place * width, width), width),
-            ] = (value * gain_ref[...] * gate).astype(BF16)
-            gather_step(head_copies[at], 0)
-
-    def head_step(step):
-        for at in orders:
-            gather_step(head_copies[at], step)
-            if step == 4:
-                inputs = hm[at // PARTS, pl.ds((at % PARTS) * part_rows, part_rows), :]
-                weights = wm_ref if at < PARTS else wm_turned
-                mix_ref[pl.ds(at * part_rows, part_rows), :] = dot(inputs, weights[...]).astype(BF16)
-
-    ticks = GROUPS + 7
-    for tick in range(ticks):
-        if tick == FINISH:
-            with jax.named_scope("prior"):
-                take_prior()
-            with jax.named_scope("heads"):
-                finish_heads()
-        for group in range(GROUPS):
-            if 0 <= tick - group < 8:
-                with jax.named_scope(f"stage{group}_{tick - group}"):
-                    stage(group, tick - group)
-            if tick == 1 and group < 2:
-                send_carry(group + 1)
-        if FINISH < tick < FINISH + 5:
-            with jax.named_scope(f"gather{tick - FINISH}"):
-                head_step(tick - FINISH)
+        rows = pl.ds(at * part_rows, part_rows)
+        queries = q_ref[rows, :]
+        own_top = top_ref[rows, 0:1]
+        top = jnp.maximum(prior_max, own_top)
+        again = jnp.exp(own_top - top)
+        carried = jnp.exp(prior_max - top) * scale
+        numerator = carried * (dot(queries, high) + dot(queries, low)) + again * num_ref[rows, :]
+        denominator = (
+            carried * jnp.sum(queries.astype(F32) * normal, axis=1, keepdims=True)
+            + again * den_ref[rows, 0:1]
+        )
+        cumulative = upright(cum_ref[0:1, at * part_rows : (at + 1) * part_rows])
+        floor = jnp.exp(-(cumulative + top))
+        value = numerator / jnp.maximum(jnp.abs(denominator), floor)
+        value = value * lax.rsqrt(jnp.mean(value * value, axis=1, keepdims=True) + EPSILON)
+        gate = jax.nn.sigmoid(og_ref[rows, :].astype(F32))
+        hm[rows, 0:width] = (value * gain_ref[...] * gate).astype(BF16)
+        for k in range(1, SIDE):
+            head_spread(at, k).start()
+
+    def mix_step(at):
+        if at == first_mixed:
+            for load in own_pieces[2 * SIDE :]:
+                load.wait()
+            for half in range(2):
+                hand_mix(half, 1 - core).wait_recv()
+        heads_of(at).wait_recv()
+        rows = pl.ds(at * part_rows, part_rows)
+        partial = dot(hm[rows, :], wmix[...])
+        mix_own[rows, :] = partial[:, 0:width]
+        for j in range(1, SIDE):
+            mix_out[j, rows, :] = partial[:, j * width : (j + 1) * width].astype(BF16)
+        for j in range(1, SIDE):
+            mix_partial(at, j).start()
+
+    def mix_finish(at):
+        mix_partials(at).wait_recv()
+        rows = pl.ds(at * part_rows, part_rows)
+        total = mix_own[rows, :]
+        for j in range(1, SIDE):
+            total = total + mix_in[j, rows, :].astype(F32)
+        mix_ref[rows, :] = total.astype(BF16)
+
+    def near_step():
+        @pl.when(core == 1)
+        def _():
+            gather_block()
+
+        send_carry(0)
+
+    first_mixed = min((SEQUENCE.index(f"m{at}"), at) for at in range(PARTS))[1]
+
+    def deal_step(at):
+        for j in range(1, SIDE):
+            deal_mix(j, at).start()
+
+    def hand_step(at):
+        mix_dealt(at).wait_recv()
+        hand_mix(at, core).start()
+
+    named_steps = {
+        "near": near_step,
+        "heads": take_prior,
+        "build": build_down,
+        "carry1": lambda: send_carry(1),
+        "carry2": lambda: send_carry(2),
+    }
+    for item in SEQUENCE:
+        with jax.named_scope(item):
+            if item in named_steps:
+                named_steps[item]()
+            elif item[0] == "s":
+                stage(int(item[1]), int(item[2]))
+            elif item[0] == "d":
+                deal_step(int(item[1]))
+            elif item[0] == "h" and item != "heads":
+                hand_step(int(item[1]))
+            elif item[0] == "g":
+                finish_heads(int(item[1]))
+            elif item[0] == "m":
+                mix_step(int(item[1]))
+            else:
+                mix_finish(int(item[1]))
     ret[0:cap, :] = outb[0:cap, :]
 
     total = jnp.zeros((tokens, width), F32)
     places = lax.broadcasted_iota(jnp.int32, (span, tokens), 0)
-    loads[11].wait()
+    loads[10].wait()
     weights = [upright(weight_ref[route : route + 1, :]) for route in range(weight_ref.shape[0])]
     for group in range(GROUPS):
         with jax.named_scope(f"back{group}"):
@@ -784,11 +863,14 @@
         sent(outb.at[foreign], ret_send.at[0])
         deals().wait_send()
         sent(tok.at[:, pl.ds(0, 3 * width)], tok_send.at[0])
+        for half in range(2):
+            mix_dealt(half).wait_send()
+            hand_mix(half, core).wait_send()
         sent(part_out.at[pl.ds(1, SIDE - 1)], part_send.at[0])
         sent(sq_in.at[:, pl.ds(1, SIDE - 1)], sq_send.at[0])
         sent(hid.at[:, pl.ds(0, (tp - 1) * 2 * units)], hid_send.at[0])
-        for part in range(2):
-            sent(hm.at[part, :, pl.ds(0, (tp - 1) * width)], head_send.at[0])
+        sent(hm.at[:, pl.ds(0, (SIDE - 1) * width)], head_send.at[0])
+        sent(mix_in.at[pl.ds(1, SIDE - 1)], mix_send.at[0])
 
     @pl.when(core == 0)
     def _():
@@ -841,7 +923,7 @@
     gate_local, up_local, down_local = gate_weight[0], up_weight[0], down_weight[0]
     small = (expert_input, routes.T, route_weight.T, in_gate, forget_gate, head_gain[None, :])
     big = (query_rows, key_rows, value_rows, out_gate, gate_local, up_local, down_local, mix_weight)
-    held = (query_rows, key_rows, value_rows, out_gate, down_local, mix_weight)
+    held = (query_rows, key_rows, value_rows, out_gate, down_local)
     tall = (HEAD + qk + 8, vw)
     message = (LABEL + qk, vw)
     return pl.pallas_call(
@@ -857,9 +939,9 @@
             pltpu.VMEM((fanout, token_count), jnp.int32),
             pltpu.VMEM((1, length), F32),
             pltpu.VMEM((1, length), F32),
-            pltpu.VMEM(mix_weight.shape, BF16),
             pltpu.VMEM((SIDE * 2 * units, SIDE * width), BF16),
-            pltpu.VMEM((2, tp * 2 * units, 2 * width), BF16),
+            pltpu.VMEM((SIDE * width, SIDE * width), BF16),
+            pltpu.VMEM((tp * 2 * units, 2 * width), BF16),
             pltpu.VMEM((slot_count, width), BF16),
             pltpu.VMEM((slot_count, SIDE * width), BF16),
             pltpu.VMEM((slot_count, 2 * units), F32),
@@ -870,7 +952,10 @@
             pltpu.VMEM((slot_count // 2, tp * 2 * units), BF16),
             pltpu.VMEM((slot_count, width), BF16),
             pltpu.VMEM((slot_count, width), BF16),
-            pltpu.VMEM((2, length // 2, tp * width), BF16),
+            pltpu.VMEM((length, SIDE * width), BF16),
+            pltpu.VMEM((length, width), F32),
+            pltpu.VMEM((SIDE, length, width), BF16),
+            pltpu.VMEM((SIDE, length, width), BF16),
             pltpu.VMEM((length, vw), F32),
             pltpu.VMEM((length, 128), F32),
             pltpu.VMEM((length, 128), F32),
@@ -885,24 +970,30 @@
             pltpu.VMEM((BLOCK - 1, *message), BF16),
             pltpu.VMEM(message, BF16),
             pltpu.VMEM(message, BF16),
-            dma((12,)),
-            dma((2 * SIDE,)),
-            dma((1,)),
-            dma((1,)),
+            dma((11,)),
+            dma((3 * SIDE,)),
+            dma((1,)),
+            dma((1,)),
+            dma((1,)),
+            dma((2,)),
+            dma((2,)),
+            dma((2,)),
             dma((1,)),
             dma((GROUPS,)),
             dma((1,)),
-            dma((GROUPS, 8)),
+            dma((GROUPS, 4)),
             dma((1,)),
             dma((GROUPS,)),
             dma((1,)),
             dma((GROUPS,)),
             dma((1,)),
-            dma((GROUPS, 8)),
+            dma((GROUPS, 5)),
             dma((1,)),
             dma((GROUPS,)),
             dma((1,)),
-            dma((2 * PARTS, 8)),
+            dma((PARTS,)),
+            dma((1,)),
+            dma((PARTS,)),
             dma((1,)),
             dma((1,)),
             dma((1,)),

time: 121 us -> 96.9 us (0.80)
  Pallas kernels: 117 us -> 92.8 us
    pallas_call x1, Pallas kernels: 117 us -> 92.8 us  [body(): pl.pallas_call(functools.partial(kernel, ep, tp, mix_weight.shape[0]), ou...]
where the time goes in v3:
time: 96.9 us; the launch traced here: 96.7 us
  Pallas kernels  92.8 us (96%)
  local copies, waits for them, and re-layouts  3.24 us (3%)
    pallas_call x1, Pallas kernels, body(): pl.pallas_call(functools.partial(kernel, ep, tp, mix_weight.shape[0]), ou...  92.8 us
    unnamed x2, local copies, waits for them, and re-layouts  3.24 us

profile of v3, /device:TPU:1, one launch (start us, length us, event | category | flops | bytes accessed | tf_op | source)
XLA Modules:
  0.0 96.7 jit_solution(14739874066246582193)
XLA Ops:
  0.6 92.8 %shard_map.149 = (bf16[512,256]{1,0:T(8,128)(2,1)}, bf16[256,256]{1,0:T(8,128)(2,1)}) custom-call(bf16[256,256]{1,0:T(8,128)(2,1)} %x_hbm.1, s32[2,256]{1,0:T(2,128)} %bitcast.9, f32[2,256]{1,0:T(2,128)} %bitcast.10, f32[1,512]{1,0:T(1,128)} %in_hbm.1, f32[1,512]{1,0:T(1,128)} %forget_hbm.1, f32[1,256]{1,0:T(1,128)} %bitcast.11, bf16[512,128]{1,0:T(8,128)(2,1)} %q_hbm.1, ...), custom_call_target="tpu_custom_call" | custom-call | tf_op jit(solution)/shard_map/pallas_call | solution.py:929
  93.5 1.7 %copy.18 = bf16[512,256]{1,0:T(8,128)(2,1)} copy(bf16[512,256]{1,0:T(8,128)(2,1)} %get-tuple-element.4) | data formatting | bytes 524288
  95.1 1.6 %copy.19 = bf16[256,256]{1,0:T(8,128)(2,1)} copy(bf16[256,256]{1,0:T(8,128)(2,1)} %get-tuple-element.5) | data formatting | bytes 262144

commit v4 on v3

--- a/solution.py
+++ b/solution.py
@@ -11,19 +11,23 @@
 LOG_FLOOR = -1e30
 F32 = jnp.float32
 BF16 = jnp.bfloat16
-GROUPS = 4
+GROUPS = 8
 SIDE = 4
 PARTS = 4
 BLOCK = 4
 HEAD = 8
 LABEL = 16
 SEQUENCE = (
-    "s00", "d0", "s01", "s10", "h0", "s02", "s20", "s11", "near", "s03", "s21", "s30", "s12",
-    "carry1", "s04", "s22", "s31", "build", "s13", "s05", "carry2", "s23", "s14", "s32", "s24",
-    "s06", "d1", "heads", "s15", "g0", "s33", "s25", "s16", "g1", "s34", "g2", "h1", "g3", "m0",
-    "s26", "s35", "m1", "m2", "m3", "s36", "f0", "f1", "f2", "f3",
+    "s00", "d0", "s01", "s10", "s20", "s02", "s11", "near", "s30", "s21", "s40", "s12", "s50",
+    "s03", "s31", "s70", "s60", "s22", "carry1", "s13", "s51", "s32", "h0", "s04", "s41", "up",
+    "s23", "carry2", "s61", "s14", "s33", "s05", "s24", "s71", "s42", "s52", "s62", "s15",
+    "heads", "s34", "s06", "g0", "s43", "s72", "s25", "s16", "g1", "s53", "g3", "s63", "d1",
+    "s44", "s35", "s26", "s54", "s73", "r0", "s45", "r3", "s36", "s64", "s55", "r1", "h1",
+    "s74", "g2", "m0", "s46", "s65", "m1", "s56", "s75", "r2", "m3", "s66", "s76", "m2", "b0",
+    "b2", "b1", "f0", "b4", "b3", "f3", "f1", "f2", "b5", "b6", "b7",
 )
-ORDER = (0, 3, -3, 4, 8, 7, -7, -6, 6, 5, -5, -4, 2, 1, -1, -2)
+TURNED = ()
+ORDER = (0, 8, 7, -7, 6, -6, 5, -5, 4, -4, 3, -3, 2, -2, 1, -1)
 
 
 def flip(index, bits):
@@ -102,6 +106,7 @@
     hid,
     outb,
     ret,
+    total_ref,
     hm,
     mix_own,
     mix_out,
@@ -332,7 +337,7 @@
             device_id={"ep": flip(me, 1)},
         )
 
-    for i in range(1, ep):
+    for i in range(1, ep // 2):
         dispatch(i).start()
 
     tok[0:cap, 0:width] = slots[0:cap, :]
@@ -446,6 +451,9 @@
             def _():
                 near(ahead).start()
 
+    for i in range(ep // 2, ep):
+        dispatch(i).start()
+
     def gather_block():
         earlier[0:HEAD, 0:qk] = jnp.zeros((HEAD, qk), F32)
         earlier[0:HEAD, qk:vw] = jnp.full((HEAD, vw - qk), LOG_FLOOR, F32)
@@ -500,13 +508,15 @@
     def build_down():
         loads[7].wait()
         nothing = jnp.zeros((units, width), BF16)
-        for at in range(tp):
-            kept = wd_ref[at * units : (at + 1) * units, :]
-            first = at * 2 * units
-            w2[first : first + units, 0:width] = kept
-            w2[first : first + units, width : 2 * width] = nothing
-            w2[first + units : first + 2 * units, 0:width] = nothing
-            w2[first + units : first + 2 * units, width : 2 * width] = kept
+        for turned in range(2 if TURNED else 1):
+            for at in range(tp):
+                unit = (at % SIDE) * SIDE + at // SIDE if turned else at
+                kept = wd_ref[unit * units : (unit + 1) * units, :]
+                first = at * 2 * units
+                w2[turned, first : first + units, 0:width] = kept
+                w2[turned, first : first + units, width : 2 * width] = nothing
+                w2[turned, first + units : first + 2 * units, 0:width] = nothing
+                w2[turned, first + units : first + 2 * units, width : 2 * width] = kept
 
 
     def spread(group, k):
@@ -571,34 +581,42 @@
             pl.ds(pl.multiple_of(at * 2 * units, 2 * units), count * 2 * units),
         ]
 
+    def axes_of(group):
+        return (row, column, SIDE, 1) if group in TURNED else (column, row, 1, SIDE)
+
     def hid_inner(group, k):
-        block_of = hid_block(group, mine, 1)
-        return pltpu.make_async_remote_copy(
-            block_of, block_of, hid_send.at[0], hid_recv.at[group, 0], device_id={"tp": flip(mine, k)}
+        inner, outer, stride, _ = axes_of(group)
+        block_of = hid_block(group, outer * SIDE + inner, 1)
+        return pltpu.make_async_remote_copy(
+            block_of, block_of, hid_send.at[0], hid_recv.at[group, 0], device_id={"tp": flip(mine, stride * k)}
         )
 
     def hid_outer(group, k):
-        block_of = hid_block(group, row * SIDE, SIDE)
+        _, outer, _, stride = axes_of(group)
+        block_of = hid_block(group, outer * SIDE, SIDE)
         return pltpu.make_async_remote_copy(
             block_of,
             block_of,
             hid_send.at[0],
             hid_recv.at[group, 1 + k // 2],
-            device_id={"tp": flip(mine, SIDE * k)},
+            device_id={"tp": flip(mine, stride * k)},
         )
 
     def hid_onward(group, k):
+        _, outer, _, stride = axes_of(group)
         quarter = half_span // 2
         block_of = hid.at[
             pl.ds(group * half_span + (k // 2) * quarter, quarter),
-            pl.ds(pl.multiple_of(flip(row, k) * SIDE * 2 * units, SIDE * 2 * units), SIDE * 2 * units),
+            pl.ds(
+                pl.multiple_of(flip(outer, k) * SIDE * 2 * units, SIDE * 2 * units), SIDE * 2 * units
+            ),
         ]
         return pltpu.make_async_remote_copy(
             block_of,
             block_of,
             hid_send.at[0],
             hid_recv.at[group, 3 + k // 2],
-            device_id={"tp": flip(mine, SIDE * (SIDE - k))},
+            device_id={"tp": flip(mine, stride * (SIDE - k))},
         )
 
     def hid_row(group):
@@ -668,7 +686,9 @@
             turned = pltpu.roll(hidden, units, 1)
             lanes = lax.broadcasted_iota(jnp.int32, (half_span, 2 * units), 1)
             both_rows = jnp.where(lanes < units, hidden[0:half_span, :], turned[half_span:span, :])
-            columns = pl.ds(pl.multiple_of(mine * 2 * units, 2 * units), 2 * units)
+            inner, outer, _, _ = axes_of(group)
+            place = outer * SIDE + inner
+            columns = pl.ds(pl.multiple_of(place * 2 * units, 2 * units), 2 * units)
             hid[packed, columns] = both_rows.astype(BF16)
             for k in range(1, SIDE):
                 hid_inner(group, k).start()
@@ -683,11 +703,13 @@
         else:
             for k in (1, 3):
                 hid_onward(group, k).wait_recv()
-            total = dot(hid[packed, :], w2[...])
+            total = dot(hid[packed, :], w2[int(group in TURNED)])
             outb[pl.ds(group * span, half_span), :] = total[:, 0:width].astype(BF16)
             outb[pl.ds(group * span + half_span, half_span), :] = total[:, width:].astype(BF16)
             for i in range(max(1, group * per), (group + 1) * per):
                 give_back(i).start()
+            if group == 0:
+                ret[0:cap, :] = outb[0:cap, :]
 
     part_rows = length // PARTS
 
@@ -697,15 +719,25 @@
             hm.at[rows, pl.ds(0, width)],
             hm.at[rows, pl.ds(k * width, width)],
             head_send.at[0],
-            head_recv.at[at],
+            head_recv.at[at, k // 2],
             device_id={"tp": flip(mine, SIDE * k)},
         )
 
-    def heads_of(at):
-        foreign = hm.at[pl.ds(at * part_rows, part_rows), pl.ds(width, (SIDE - 1) * width)]
-        return pltpu.make_async_remote_copy(
-            foreign, foreign, head_send.at[0], head_recv.at[at], device_id={"tp": flip(mine, 1)}
-        )
+    def head_onward(at, k):
+        half = part_rows // 2
+        rows = pl.ds(at * part_rows + (k // 2) * half, half)
+        return pltpu.make_async_remote_copy(
+            hm.at[rows, pl.ds(k * width, width)],
+            hm.at[rows, pl.ds(2 * width, width)],
+            head_send.at[0],
+            head_recv.at[at, 2 + k // 2],
+            device_id={"tp": flip(mine, SIDE * (SIDE - k))},
+        )
+
+    def relay_heads(at):
+        for k in (1, 3):
+            head_spread(at, k).wait_recv()
+            head_onward(at, k).start()
 
     def mix_partial(at, j):
         rows = pl.ds(at * part_rows, part_rows)
@@ -770,7 +802,7 @@
         value = value * lax.rsqrt(jnp.mean(value * value, axis=1, keepdims=True) + EPSILON)
         gate = jax.nn.sigmoid(og_ref[rows, :].astype(F32))
         hm[rows, 0:width] = (value * gain_ref[...] * gate).astype(BF16)
-        for k in range(1, SIDE):
+        for k in (1, 3):
             head_spread(at, k).start()
 
     def mix_step(at):
@@ -779,7 +811,8 @@
                 load.wait()
             for half in range(2):
                 hand_mix(half, 1 - core).wait_recv()
-        heads_of(at).wait_recv()
+        for k in (1, 3):
+            head_onward(at, k).wait_recv()
         rows = pl.ds(at * part_rows, part_rows)
         partial = dot(hm[rows, :], wmix[...])
         mix_own[rows, :] = partial[:, 0:width]
@@ -803,6 +836,7 @@
 
         send_carry(0)
 
+    first_back = min((SEQUENCE.index(f"b{at}"), at) for at in range(GROUPS))[1]
     first_mixed = min((SEQUENCE.index(f"m{at}"), at) for at in range(PARTS))[1]
 
     def deal_step(at):
@@ -813,10 +847,25 @@
         mix_dealt(at).wait_recv()
         hand_mix(at, core).start()
 
+    def back_step(group):
+        if group == first_back:
+            loads[10].wait()
+        given_back(group).wait_recv()
+        rows = pl.ds(group * span, span)
+        places = lax.broadcasted_iota(jnp.int32, (span, tokens), 0)
+        for route in range(2):
+            hit = places == slot_row_ref[route : route + 1, :] - group * span
+            picked = dot(hit.astype(F32).astype(BF16), ret[rows, :], ((0,), (0,)))
+            picked = picked * upright(weight_ref[route : route + 1, :])
+            if group == first_back and route == 0:
+                total_ref[...] = picked
+            else:
+                total_ref[...] += picked
+
     named_steps = {
         "near": near_step,
         "heads": take_prior,
-        "build": build_down,
+        "up": build_down,
         "carry1": lambda: send_carry(1),
         "carry2": lambda: send_carry(2),
     }
@@ -830,27 +879,17 @@
                 deal_step(int(item[1]))
             elif item[0] == "h" and item != "heads":
                 hand_step(int(item[1]))
+            elif item[0] == "b":
+                back_step(int(item[1]))
             elif item[0] == "g":
                 finish_heads(int(item[1]))
+            elif item[0] == "r":
+                relay_heads(int(item[1]))
             elif item[0] == "m":
                 mix_step(int(item[1]))
             else:
                 mix_finish(int(item[1]))
-    ret[0:cap, :] = outb[0:cap, :]
-
-    total = jnp.zeros((tokens, width), F32)
-    places = lax.broadcasted_iota(jnp.int32, (span, tokens), 0)
-    loads[10].wait()
-    weights = [upright(weight_ref[route : route + 1, :]) for route in range(weight_ref.shape[0])]
-    for group in range(GROUPS):
-        with jax.named_scope(f"back{group}"):
-            given_back(group).wait_recv()
-        rows = pl.ds(group * span, span)
-        for route, weight in enumerate(weights):
-            hit = places == slot_row_ref[route : route + 1, :] - group * span
-            picked = dot(hit.astype(F32).astype(BF16), ret[rows, :], ((0,), (0,)))
-            total += picked * weight
-    exp_ref[...] = total.astype(BF16)
+    exp_ref[...] = total_ref[...].astype(BF16)
 
     def sent(source, semaphore):
         pltpu.make_async_remote_copy(
@@ -926,11 +965,11 @@
     held = (query_rows, key_rows, value_rows, out_gate, down_local)
     tall = (HEAD + qk + 8, vw)
     message = (LABEL + qk, vw)
-    return pl.pallas_call(
+    results = pl.pallas_call(
         functools.partial(kernel, ep, tp, mix_weight.shape[0]),
         out_shape=(
-            jax.ShapeDtypeStruct((length, width), BF16),
-            jax.ShapeDtypeStruct((token_count, width), BF16),
+            pltpu.VMEM((length, width), BF16),
+            pltpu.VMEM((token_count, width), BF16),
         ),
         in_specs=[anywhere] * 14,
         out_specs=(vmem, vmem),
@@ -941,7 +980,7 @@
             pltpu.VMEM((1, length), F32),
             pltpu.VMEM((SIDE * 2 * units, SIDE * width), BF16),
             pltpu.VMEM((SIDE * width, SIDE * width), BF16),
-            pltpu.VMEM((tp * 2 * units, 2 * width), BF16),
+            pltpu.VMEM((2 if TURNED else 1, tp * 2 * units, 2 * width), BF16),
             pltpu.VMEM((slot_count, width), BF16),
             pltpu.VMEM((slot_count, SIDE * width), BF16),
             pltpu.VMEM((slot_count, 2 * units), F32),
@@ -952,6 +991,7 @@
             pltpu.VMEM((slot_count // 2, tp * 2 * units), BF16),
             pltpu.VMEM((slot_count, width), BF16),
             pltpu.VMEM((slot_count, width), BF16),
+            pltpu.VMEM((token_count, width), F32),
             pltpu.VMEM((length, SIDE * width), BF16),
             pltpu.VMEM((length, width), F32),
             pltpu.VMEM((SIDE, length, width), BF16),
@@ -991,7 +1031,7 @@
             dma((1,)),
             dma((GROUPS,)),
             dma((1,)),
-            dma((PARTS,)),
+            dma((PARTS, 4)),
             dma((1,)),
             dma((PARTS,)),
             dma((1,)),
@@ -1007,6 +1047,7 @@
             collective_id=0, has_side_effects=True, vmem_limit_bytes=64000 * 1024
         ),
     )(*small, *big)
+    return results
 
 
 def solution(mesh):

time: 96.9 us -> 91.7 us (0.946)
  Pallas kernels: 92.8 us -> 89.5 us
  local copies, waits for them, and re-layouts: 3.24 us -> 1.36 us
    pallas_call x1, Pallas kernels: 92.8 us -> 89.5 us  [body(): pl.pallas_call(functools.partial(kernel, ep, tp, mix_weight.shape[0]), ou...]
    unnamed x2, local copies, waits for them, and re-layouts: 3.24 us -> 1.36 us
where the time goes in v4:
time: 91.7 us; the launch traced here: 91.5 us
  Pallas kernels  89.5 us (98%)
  local copies, waits for them, and re-layouts  1.36 us (1%)
    pallas_call x1, Pallas kernels, body(): pl.pallas_call(functools.partial(kernel, ep, tp, mix_weight.shape[0]), ou...  89.5 us

profile of v4, /device:TPU:1, one launch (start us, length us, event | category | flops | bytes accessed | tf_op | source)
XLA Modules:
  0.0 91.5 jit_solution(7917422606610568688)
XLA Ops:
  0.6 89.5 %shard_map.149 = (bf16[512,256]{1,0:T(8,128)(2,1)S(1)}, bf16[256,256]{1,0:T(8,128)(2,1)S(1)}) custom-call(bf16[256,256]{1,0:T(8,128)(2,1)} %x_hbm.1, s32[2,256]{1,0:T(2,128)} %bitcast.9, f32[2,256]{1,0:T(2,128)} %bitcast.10, f32[1,512]{1,0:T(1,128)} %in_hbm.1, f32[1,512]{1,0:T(1,128)} %forget_hbm.1, f32[1,256]{1,0:T(1,128)} %bitcast.11, ...), custom_call_target="tpu_custom_call" | custom-call | tf_op jit(solution)/shard_map/pallas_call | solution.py:968
  90.1 0.7 copy.18
  90.8 0.7 copy.19
